TPU v7x, 128 devices: a whole 4x4x4 slice. The times are simulated.
128 devices in a mesh: sp: 32 (over z, y, core), tp: 4 (over x).
Axes of the slice: x: 4, y: 4, z: 4, core: 2. Of those that a mesh axis runs over, the one named last changes fastest.
Arguments:
- layer_input: bfloat16 [24576, 2048], P('sp', 'tp'), may hold values from -6 to 6
- input_norm_gain: bfloat16 [2048], replicated, may hold values from 0.099609375 to 1.8984375
- query_weight: bfloat16 [2048, 2048], P(None, 'tp'), may hold values from -0.125 to 0.125
- forget_weight: bfloat16 [2048, 2048], P(None, 'tp'), may hold values from -0.125 to 0.125
- value_matrix: bfloat16 [2048, 2048], P(None, 'tp'), may hold values from -0.125 to 0.125
- output_gate_weight: bfloat16 [2048, 2048], P(None, 'tp'), may hold values from -0.125 to 0.125
- after_gate_weight: bfloat16 [2048, 2048], P(None, 'tp'), may hold values from -0.125 to 0.125
- before_gate_weight: bfloat16 [2048, 2048], P(None, 'tp'), may hold values from -0.125 to 0.125
- convolution_input_weight: bfloat16 [2048, 2048], P(None, 'tp'), may hold values from -0.125 to 0.125
- forget_minimum: float32 [2048], P('tp'), may hold values from 0.95 to 0.99999593
- surge_log_decay: float32 [24576, 2048], P('sp', 'tp'), may hold values from -2.2 to 0
- convolution_kernel: bfloat16 [3, 2048], P(None, 'tp'), may hold values from -4 to 4
- head_norm_gain: bfloat16 [128], replicated, may hold values from 0.099609375 to 1.8984375
- starting_state: float32 [16, 128, 128], P('tp', 'sp'), may hold values from -0.046875 to 0.046875
- recurrence_output_weight: bfloat16 [2048, 2048], P('tp'), may hold values from -0.09375 to 0.09375
- convolution_output_weight: bfloat16 [2048, 2048], P('tp'), may hold values from -0.09375 to 0.09375
- output_norm_gain: bfloat16 [2048], replicated, may hold values from 0.099609375 to 1.8984375
Outputs:
- layer_out: bfloat16 [24576, 2048], P(('sp', 'tp'))
All inputs are finite; a program needn't handle non-finite values.
Results may differ from a plain program's by a relative error of at most 0.014.
Values may be sent and summed in bfloat16 or wider, within the bound.
A program may use at most 128 MiB of HBM per device.

v0:
```python
import jax
import jax.numpy as jnp
from jax import lax
from jax.sharding import Mesh
from jax.sharding import PartitionSpec as P

D = 2048
DK = 128
DV = 128
CK = 3
BLK = 64
SP = ("sp_0", "sp_1", "sp_2")
SP_TP = ("sp_0", "sp_1", "sp_2", "tp")


EPS = 1e-06
PRECISE_PRODUCT = lax.Precision.HIGHEST


def in_one_piece(arrays, axis, split_dim, concat_dim, along):
    widths = [a.shape[along] for a in arrays]
    both = jnp.concatenate(arrays, axis=along)
    whole = lax.all_to_all(both, axis, split_axis=split_dim, concat_axis=concat_dim, tiled=True)
    return tuple(jnp.split(whole, [sum(widths[:k]) for k in range(1, len(widths))], axis=along))


def split_up(value, dim, peers):
    before, after = (value.shape[:dim], value.shape[dim + 1 :])
    return jnp.moveaxis(value.reshape(*before, peers, -1, *after), dim, 0)


def in_order(pieces, dim):
    shape = list(pieces.shape[1:])
    shape[dim] *= pieces.shape[0]
    return jnp.moveaxis(pieces, 0, dim).reshape(shape)


def exchange_in_order(pieces, axes, turns):
    shape = [lax.axis_size(a) for a in axes]
    pieces = pieces.reshape(*shape, *pieces.shape[1:])
    for k in turns:
        pieces = lax.all_to_all(pieces, axes[k], split_axis=k, concat_axis=k, tiled=True)
    return pieces.reshape(-1, *pieces.shape[len(axes) :])


def two_step_exchange(value, groups, turns, split_dim, concat_dim):
    peers = lax.axis_size(groups[0]) * lax.axis_size(groups[1])
    pieces = split_up(value, split_dim, peers)
    return in_order(exchange_in_order(pieces, groups, turns), concat_dim)


def from_behind(value, axis, by):
    peers = lax.axis_size(axis)
    pairs = [(i, i + by) for i in range(peers) if 0 <= i + by < peers]
    return lax.ppermute(value, axis, pairs)


def rms_scale(value_rows):
    return lax.rsqrt(jnp.mean(value_rows * value_rows, axis=-1, keepdims=True) + EPS)


def block_pass(carry, inputs):
    latent_state, running = carry
    query_rows, key_inputs, value_rows, forget_gate_logits = inputs
    cumulative_decay = jnp.cumsum(forget_gate_logits, axis=1)
    length = query_rows.shape[1]
    causal_masking = jnp.tril(jnp.ones((length, length), dtype=bool))[None, :, :]
    query_scaled_rows = query_rows * jnp.exp(cumulative_decay)
    scaled_key = key_inputs * jnp.exp(-cumulative_decay)
    crossed_output = jnp.einsum(
        "bqy,byx->bqx", query_scaled_rows, latent_state, precision=PRECISE_PRODUCT
    )
    scores = jnp.einsum("htk,hsk->hts", query_scaled_rows, scaled_key, precision=PRECISE_PRODUCT)
    scores = jnp.where(causal_masking, scores, 0.0)
    o_intra = jnp.einsum("hts,hsv->htv", scores, value_rows, precision=PRECISE_PRODUCT)
    block_total = cumulative_decay[:, -1, :]
    latent_state = jnp.exp(block_total)[..., None] * latent_state + jnp.einsum(
        "otm,ote->ome",
        scaled_key * jnp.exp(block_total)[:, None, :],
        value_rows,
        precision=PRECISE_PRODUCT,
    )
    shifted = query_scaled_rows * jnp.exp(running)[:, None, :]
    return ((latent_state, running + block_total), (o_intra + crossed_output, shifted))


def shards(
    layer_input,
    input_norm_gain,
    query_weight,
    forget_weight,
    value_matrix,
    output_gate_weight,
    after_gate_weight,
    before_gate_weight,
    convolution_input_weight,
    forget_minimum,
    surge_log_decay,
    convolution_kernel,
    head_norm_gain,
    starting_state,
    recurrence_output_weight,
    convolution_output_weight,
    output_norm_gain,
):
    tokens_dev = layer_input.shape[0]
    heads_local = query_weight.shape[1] // DK
    blocks = tokens_dev // BLK
    weight_list = (
        query_weight,
        forget_weight,
        value_matrix,
        output_gate_weight,
        after_gate_weight,
        before_gate_weight,
        convolution_input_weight,
    )
    local_rows = layer_input.astype(jnp.float32)
    squares = lax.psum(jnp.sum(local_rows * local_rows, axis=1), "tp")
    row_scale = lax.rsqrt(squares / D + EPS)
    width_local = layer_input.shape[1]
    gain_local = lax.dynamic_slice_in_dim(
        input_norm_gain, lax.axis_index("tp") * width_local, width_local
    )
    normed_local = (local_rows * row_scale[:, None] * gain_local.astype(jnp.float32)).astype(
        jnp.bfloat16
    )
    piece = lax.all_gather(normed_local, "tp", axis=1, tiled=True)
    summed = tuple(
        (jnp.dot(piece, weight, preferred_element_type=jnp.float32) for weight in weight_list)
    )
    projections = tuple((total.astype(jnp.bfloat16) for total in summed))
    query_raw, forget_raw, value_raw, outgate_raw, postgate_raw, pregate_raw, convval_raw = (
        projections
    )
    forget_single = forget_raw.astype(jnp.float32)
    forget_gate_logits = (
        jnp.logaddexp(
            jnp.log(forget_minimum), jnp.log1p(-forget_minimum) + jax.nn.log_sigmoid(forget_single)
        )
        + surge_log_decay
    )
    key_inputs = (1.0 - forget_minimum) * jax.nn.sigmoid(-forget_single)
    query_rows = jax.nn.silu(query_raw.astype(jnp.float32)) * DK ** (-0.5)

    def to_blocks(value_rows, width):
        return value_rows.reshape(blocks, BLK, heads_local, width).transpose(0, 2, 1, 3)

    zero_state = jnp.zeros((heads_local, DK, DV), jnp.float32)
    zero_total = jnp.zeros((heads_local, DK), jnp.float32)
    (local_state, local_total), (partial_output, shifted_query) = lax.scan(
        block_pass,
        (zero_state, zero_total),
        (
            to_blocks(query_rows, DK),
            to_blocks(key_inputs, DK),
            to_blocks(value_raw.astype(jnp.float32), DV),
            to_blocks(forget_gate_logits, DK),
        ),
    )
    moved_state, moved_total = in_one_piece(
        (local_state[None], local_total[None, :, :, None]), SP, 2, 0, 3
    )

    def advance(running, item):
        piece_state, piece_total = item
        return (jnp.exp(piece_total) * running + piece_state, running)

    _, entering = lax.scan(advance, starting_state, (moved_state, moved_total))
    carried_state = two_step_exchange(entering, (("sp_0", "sp_1"), "sp_2"), (1, 0), 0, 2)[0]
    recurrence_step = partial_output + jnp.einsum(
        "aoxq,oqu->aoxu", shifted_query, carried_state, precision=PRECISE_PRODUCT
    )
    recurrence_step = recurrence_step.transpose(0, 2, 1, 3).reshape(tokens_dev, heads_local, DV)
    normed_heads = recurrence_step * rms_scale(recurrence_step) * head_norm_gain.astype(jnp.float32)
    rec_out = (
        normed_heads.reshape(tokens_dev, heads_local * DV)
        * jax.nn.silu(outgate_raw.astype(jnp.float32))
    ).astype(jnp.bfloat16)
    mixed_in = pregate_raw.astype(jnp.float32) * convval_raw.astype(jnp.float32)
    rim_rows = from_behind(mixed_in[tokens_dev - (CK - 1) :], SP, 1)
    padded = jnp.concatenate([rim_rows, mixed_in], axis=0)
    taps_f = convolution_kernel.astype(jnp.float32)
    conv_sum = padded[0:tokens_dev] * taps_f[0]
    for offset in range(1, CK):
        conv_sum = conv_sum + padded[offset : offset + tokens_dev] * taps_f[offset]
    conv_out = (postgate_raw.astype(jnp.float32) * conv_sum).astype(jnp.bfloat16)
    mixed = lax.psum_scatter(
        (
            jnp.dot(rec_out, recurrence_output_weight, preferred_element_type=jnp.float32)
            + jnp.dot(conv_out, convolution_output_weight, preferred_element_type=jnp.float32)
        ).astype(jnp.bfloat16),
        "tp",
        scatter_dimension=0,
        tiled=True,
    ).astype(jnp.float32)
    return (mixed * rms_scale(mixed) * output_norm_gain.astype(jnp.float32)).astype(jnp.bfloat16)


def solution(mesh):
    finer = Mesh(mesh.devices.reshape(4, 4, 2, mesh.shape["tp"]), ("sp_0", "sp_1", "sp_2", "tp"))
    in_specs = (
        P(SP, "tp"),
        P(),
        P(None, "tp"),
        P(None, "tp"),
        P(None, "tp"),
        P(None, "tp"),
        P(None, "tp"),
        P(None, "tp"),
        P(None, "tp"),
        P("tp"),
        P(SP, "tp"),
        P(None, "tp"),
        P(),
        P("tp", SP, None),
        P("tp", None),
        P("tp", None),
        P(),
    )
    out_specs = P(SP_TP, None)
    return jax.shard_map(
        shards, mesh=finer, in_specs=in_specs, out_specs=out_specs, check_vma=False
    )
```

profile of v0, /device:TPU:1, one launch (start us, length us, event | category | flops | bytes accessed | tf_op | source)
XLA Modules:
  0.0 326.3 jit_solution(134104087101304035)
XLA Ops:
  8.1 9.3 %psum.7 = f32[768]{0:T(1024)S(1)} all-reduce(f32[768]{0:T(1024)S(1)} %fusion.27), channel_id=1, replica_groups=mesh['sp_0'=4,'sp_1'=4,'sp_2'=2,'tp'=4] {'tp'}, use_global_device_ids=true, to_apply=%region_1.0 | all-reduce | flops 768 | bytes 6144 | tf_op jit(solution)/shard_map/psum | solution.py:119
  18.1 2.3 fusion.29
  20.5 41.5 %all-gather.2.cloned.1.call-done = bf16[768,2048]{1,0:T(8,128)(2,1)} async-done(((bf16[768,512]{1,0:T(8,128)(2,1)}), bf16[768,2048]{1,0:T(8,128)(2,1)}) %all-gather.2.cloned.1.call-update) | async-done | bytes 3145744 | tf_op jit(solution)/shard_map/all_gather | solution.py:128
  62.1 8.4 %fusion.36 = (f32[768,512]{1,0:T(8,128)}, f32[768,512]{1,0:T(8,128)}) fusion(f32[512]{0:T(512)S(1)} %get-tuple-element.175, f32[768,512]{1,0:T(8,128)} %param.31, f32[512]{0:T(512)S(1)} %get-tuple-element.177, f32[512]{0:T(512)S(1)} %get-tuple-element.176, bf16[768,2048]{1,0:T(8,128)(2,1)} %all-gather.2.cloned.1.call-done, bf16[2048,512]{1,0:T(8,128)(2,1)} %param.24), kind=kOutput, calls=%fused_computation.66 | convolution fusion | flops 1619656704 | bytes 9967616 | tf_op jit(solution)/shard_map/dot_general | solution.py:130
  70.4 2.7 reshape.84
  73.2 2.7 reshape.85
  75.9 5.7 %fusion.40 = f32[768,512]{1,0:T(8,128)} fusion(bf16[768,2048]{1,0:T(8,128)(2,1)} %all-gather.2.cloned.1.call-done, bf16[2048,512]{1,0:T(8,128)(2,1)} %param.23), kind=kOutput, calls=%fused_computation.70 | convolution fusion | flops 1613365248 | bytes 6815744 | tf_op jit(solution)/shard_map/dot_general | solution.py:130
  81.6 2.7 reshape.87
  84.4 5.5 %fusion.54 = f32[768,512]{1,0:T(8,128)} fusion(bf16[768,2048]{1,0:T(8,128)(2,1)} %all-gather.2.cloned.1.call-done, bf16[2048,512]{1,0:T(8,128)(2,1)} %param.25), kind=kOutput, calls=%fused_computation.100 | convolution fusion | flops 1611399168 | bytes 6815744 | tf_op jit(solution)/shard_map/dot_general | solution.py:130
  89.8 2.7 reshape.90
  92.6 4.1 %copy_bitcast_fusion.3 = (f32[12,4,64,128]{3,2,1,0:T(8,128)}, f32[12,4,64,128]{3,2,1,0:T(8,128)}) fusion(f32[12,64,4,128]{3,2,1,0:T(4,128)} %reshape.85, f32[12,64,4,128]{3,2,1,0:T(4,128)} %reshape.84), kind=kLoop, calls=%fused_computation.88 | loop fusion | bytes 6291456 | tf_op jit(solution)/shard_map/transpose | solution.py:147
  96.7 2.1 copy_bitcast_fusion.1
  98.8 105.2 %while.30 = (s32[]{:T(128)}, f32[4,128,128]{2,1,0:T(8,128)S(1)}, f32[4,128]{1,0:T(4,128)S(1)}, f32[12,4,64,128]{3,2,0,1:T(8,128)}, f32[12,4,64,128]{3,2,0,1:T(8,...) while((s32[]{:T(128)}, f32[4,128,128]{2,1,0:T(8,128)S(1)}, ...), condition=%wide.region_4.5_spmd.clone, body=%wide.region_2.4_spmd.clone.sunk | while | flops 153670656 | bytes 3577993 | solution.py:151
  104.0 1.9 fusion.95
  106.0 1.6 convolution_add_fusion.3
  112.8 1.9 fusion.95
  114.7 1.6 convolution_add_fusion.3
  121.6 1.9 fusion.95
  123.5 1.6 convolution_add_fusion.3
  130.3 1.9 fusion.95
  132.3 1.6 convolution_add_fusion.3
  139.1 1.9 fusion.95
  147.9 1.9 fusion.95
  149.8 1.6 convolution_add_fusion.3
  156.6 1.9 fusion.95
  158.6 1.6 convolution_add_fusion.3
  165.4 1.9 fusion.95
  174.2 1.9 fusion.95
  183.0 1.9 fusion.95
  191.7 1.9 fusion.95
  193.7 1.6 convolution_add_fusion.3
  200.5 1.9 fusion.95
  202.4 1.6 convolution_add_fusion.3
  205.4 7.9 %all-to-all-start = ((f32[1,4,128,129]{3,1,0,2:T(4,128)}), f32[1,4,128,129]{3,1,0,2:T(4,128)S(1)}, u32[]{:S(2)}, u32[]{:S(2)}) async-start(f32[1,4,128,129]{3,1,0,2:T(4,128)} %pad_maximum_fusion.1), calls=%async_computation | async-start | bytes 1048576 | tf_op jit(solution)/shard_map/all_to_all | solution.py:23
  213.3 5.2 %convolution_convert_fusion = bf16[768,512]{1,0:T(8,128)(2,1)} fusion(bf16[768,2048]{1,0:T(8,128)(2,1)} %all-gather.2.cloned.1.call-done, bf16[2048,512]{1,0:T(8,128)(2,1)} %param.29), kind=kOutput, calls=%fused_computation.94 | convolution fusion | flops 1611005952 | bytes 6029312 | tf_op jit(solution)/shard_map/dot_general | solution.py:130
  218.5 6.2 %all-to-all-done = f32[1,4,128,129]{3,1,0,2:T(4,128)S(1)} async-done(((f32[1,4,128,129]{3,1,0,2:T(4,128)}), f32[1,4,128,129]{3,1,0,2:T(4,128)S(1)}, u32[]{:S(2)}, u32[]{:S(2)}) %all-to-all-start) | async-done | bytes 264224 | tf_op jit(solution)/shard_map/all_to_all | solution.py:23
  225.7 3.4 %while.29 = (s32[]{:T(128)}, f32[4,4,128]{2,1,0:T(4,128)S(1)}, f32[32,4,4,128]{3,2,1,0:T(4,128)S(1)}, f32[32,4,4,1]{2,1,3,0:T(4,128)S(1)}, f32[32,4,4,128]{3,1,2,0:T(4,128)S(1)}, /*index=5*/s32[]{:T(128)}) while((s32[]{:T(128)}, f32[4,4,128]{2,1,0:T(4,128)S(1)}, f32[32,4,4,128]{3,2,1,0:T(4,128)S(1)}, f32[32,4,4,1]{2,1,3,0:T(4,128)S(1)}, ...), condition=%wide.region_6.7_spmd, body=%wide.region_5.6_spmd.sunk | while | flops 4098 | bytes 57617 | solution.py:169
  229.1 4.1 %all_to_all.28 = f32[16,2,1,4,4,128]{5,4,3,0,2,1:T(4,128)S(1)} all-to-all(f32[16,2,1,4,4,128]{5,4,3,0,2,1:T(4,128)S(1)} %copy.64), channel_id=1, replica_groups=mesh['sp_0'=4,'sp_1'=4,'sp_2'=2,'tp'=4] {'sp_2'}, dimensions={1} | all-to-all | bytes 524288 | tf_op jit(solution)/shard_map/all_to_all | solution.py:42
  233.9 3.5 %all-to-all-start.2 = ((f32[16,2,1,4,4,128]{5,4,3,1,2,0:T(4,128)}), f32[16,2,1,4,4,128]{5,4,3,1,2,0:T(4,128)S(1)}, u32[]{:S(2)}, u32[]{:S(2)}) async-start(f32[16,2,1,4,4,128]{5,4,3,1,2,0:T(4,128)} %copy.65), calls=%async_computation.2 | async-start | bytes 524288 | tf_op jit(solution)/shard_map/all_to_all | solution.py:42
  237.5 4.3 %convert_multiply_fusion.6 = f32[768,512]{1,0:T(8,128)S(1)} fusion(bf16[768,512]{1,0:T(8,128)(2,1)S(1)} %copy-done.9, bf16[768,2048]{1,0:T(8,128)(2,1)} %all-gather.2.cloned.1.call-done, bf16[2048,512]{1,0:T(8,128)(2,1)} %param.28), kind=kOutput, calls=%fused_computation.90 | convolution fusion | flops 1612185600 | bytes 7602176 | tf_op jit(solution)/shard_map/dot_general | solution.py:130
  243.0 3.7 %collective-permute-start = (f32[2,512]{1,0:T(2,128)S(1)}, f32[2,512]{1,0:T(2,128)S(1)}, u32[]{:S(2)}, u32[]{:S(2)}) collective-permute-start(f32[2,512]{1,0:T(2,128)S(1)} %slice.29), channel_id=1, source_target_pairs={{0,4},{4,8},{8,12},{12,16},{16,20},{20,24},{24,28},{28,32},{32,36}... | collective-permute-start | bytes 12296 | tf_op jit(solution)/shard_map/ppermute | solution.py:55
  246.8 4.5 %multiply_reduce_fusion = (f32[12,64,4]{1,0,2:T(8,128)S(1)}, f32[12,64,4,128]{3,1,0,2:T(8,128)}) fusion(f32[12,4,64,128]{3,2,0,1:T(8,128)} %get-tuple-element.82, f32[4,128,128,1]{2,1,3,0:T(8,128)S(1)} %bitcast.154, f32[12,4,64,128]{3,2,0,1:T(8,128)} %get-tuple-element.86), kind=kOutput, calls=%fused_computation.91 | convolution fusion | flops 605156352 | bytes 4993024 | tf_op jit(solution)/shard_map/aoxq,oqu->aoxu/dot_general | solution.py:171
  251.5 3.6 %copy.69 = f32[12,64,4,128]{3,2,1,0:T(4,128)} copy(f32[12,64,4,128]{3,1,0,2:T(8,128)} %get-tuple-element.179) | data formatting | bytes 3145728 | tf_op jit(solution)/shard_map/transpose | solution.py:174
  255.1 1.9 mul.185
  256.9 9.7 %fusion.55 = f32[768,2048]{1,0:T(8,128)} fusion(bf16[512,2048]{1,0:T(8,128)(2,1)S(1)} %copy-done, f32[96,8,4,128]{3,2,1,0:T(4,128)} %bitcast.152, f32[96,8,4,128]{3,2,1,0:T(4,128)} %bitcast.151, bf16[768,2048]{1,0:T(8,128)(2,1)} %all-gather.2.cloned.1.call-done, bf16[2048,512]{1,0:T(8,128)(2,1)} %param.26, f32[512]{0:T(512)S(1)} %broadcast_bitcast_fusion), kind=kOutput, calls=%fused_computation.102 | convolution fusion | flops 3225157632 | bytes 16779264 | tf_op jit(solution)/shard_map/dot_general | solution.py:190
  266.6 11.6 %add_convert_fusion = bf16[768,2048]{1,0:T(8,128)(2,1)} fusion(f32[768,2048]{1,0:T(8,128)} %fusion.55, bf16[512,2048]{1,0:T(8,128)(2,1)} %param.36, f32[2,512]{1,0:T(2,128)S(1)} %collective-permute-done, f32[768,512]{1,0:T(8,128)} %copy-done.7, bf16[768,2048]{1,0:T(8,128)(2,1)} %all-gather.2.cloned.1.call-done, bf16[2048,512]{1,0:T(8,128)(2,1)} %param.27, ...), kind=kOutput, calls=%fused_computation.35 | convolution fusion | flops 3228696576 | bytes 18360320 | tf_op jit(solution)/shard_map/dot_general | solution.py:191
  278.9 36.9 %reduce-scatter.2.cloned.1.call-done = bf16[192,2048]{1,0:T(8,128)(2,1)} async-done(((bf16[768,2048]{1,0:T(8,128)(2,1)}), bf16[192,2048]{1,0:T(8,128)(2,1)}) %reduce-scatter.2.cloned.1.call-update) | async-done | bytes 786448 | tf_op jit(solution)/shard_map/reduce_scatter | solution.py:188
  317.2 2.3 fusion.47
  (281 shorter events, 80.4 us)
Async XLA Ops:
  6.5 250.4 %copy-start = (bf16[512,2048]{1,0:T(8,128)(2,1)S(1)}, bf16[512,2048]{1,0:T(8,128)(2,1)}, u32[]{:S(2)}) copy-start(bf16[512,2048]{1,0:T(8,128)(2,1)} %param.35) | copy-start | bytes 6291460
  6.5 55.5 %all-gather.2.cloned.1.call-start = ((), (), s32[]{:S(2)}) async-start(), calls=%async_computation.4 | async-start | bytes 3932160 | tf_op jit(solution)/shard_map/all_gather | solution.py:128
  6.5 13.9 %copy-start.8 = (bf16[128]{0:T(256)(128)(2,1)S(1)}, bf16[128]{0:T(256)(128)(2,1)}, u32[]{:S(2)}) copy-start(bf16[128]{0:T(256)(128)(2,1)} %param.33) | copy-start | bytes 772
  6.5 13.9 %copy-start.6 = (f32[512]{0:T(512)S(1)}, f32[512]{0:T(512)}, u32[]{:S(2)}) copy-start(f32[512]{0:T(512)} %param.30) | copy-start | bytes 6148
  6.5 14.0 %copy-start.4 = (bf16[3,512]{1,0:T(4,128)(2,1)S(1)}, bf16[3,512]{1,0:T(4,128)(2,1)}, u32[]{:S(2)}) copy-start(bf16[3,512]{1,0:T(4,128)(2,1)} %param.32) | copy-start | bytes 9220
  92.6 4.1 %copy-start.1 = (f32[12,64,4,128]{3,2,1,0:T(4,128)S(1)}, f32[12,64,4,128]{3,2,1,0:T(4,128)}, u32[]{:S(2)}) copy-start(f32[12,64,4,128]{3,2,1,0:T(4,128)} %reshape.87) | copy-start | bytes 4718596
  92.6 4.1 %copy-start.2 = (f32[12,64,4,128]{3,2,1,0:T(4,128)S(1)}, f32[12,64,4,128]{3,2,1,0:T(4,128)}, u32[]{:S(2)}) copy-start(f32[12,64,4,128]{3,2,1,0:T(4,128)} %reshape.90) | copy-start | bytes 4718596
  205.4 19.3 %all-to-all-start = ((f32[1,4,128,129]{3,1,0,2:T(4,128)}), f32[1,4,128,129]{3,1,0,2:T(4,128)S(1)}, u32[]{:S(2)}, u32[]{:S(2)}) async-start(f32[1,4,128,129]{3,1,0,2:T(4,128)} %pad_maximum_fusion.1), calls=%async_computation | async-start | bytes 1048576 | tf_op jit(solution)/shard_map/all_to_all | solution.py:23
  213.2 12.4 %copy-start.3 = (f32[4,4,128]{2,1,0:T(4,128)S(1)}, f32[4,4,128]{2,1,0:T(4,128)}, u32[]{:S(2)}) copy-start(f32[4,4,128]{2,1,0:T(4,128)} %param.34) | copy-start | bytes 24580
  229.1 8.4 %copy-start.9 = (bf16[768,512]{1,0:T(8,128)(2,1)S(1)}, bf16[768,512]{1,0:T(8,128)(2,1)}, u32[]{:S(2)}) copy-start(bf16[768,512]{1,0:T(8,128)(2,1)} %convolution_convert_fusion) | copy-start | bytes 2359300
  233.9 12.8 %all-to-all-start.2 = ((f32[16,2,1,4,4,128]{5,4,3,1,2,0:T(4,128)}), f32[16,2,1,4,4,128]{5,4,3,1,2,0:T(4,128)S(1)}, u32[]{:S(2)}, u32[]{:S(2)}) async-start(f32[16,2,1,4,4,128]{5,4,3,1,2,0:T(4,128)} %copy.65), calls=%async_computation.2 | async-start | bytes 524288 | tf_op jit(solution)/shard_map/all_to_all | solution.py:42
  237.5 78.4 %reduce-scatter.2.cloned.1.call-start = ((), (), s32[]{:S(2)}) async-start(), calls=%async_computation.5 | async-start | bytes 3932160 | tf_op jit(solution)/shard_map/reduce_scatter | solution.py:188
  241.9 1.2 copy-start.7
  243.0 23.6 %collective-permute-start = (f32[2,512]{1,0:T(2,128)S(1)}, f32[2,512]{1,0:T(2,128)S(1)}, u32[]{:S(2)}, u32[]{:S(2)}) collective-permute-start(f32[2,512]{1,0:T(2,128)S(1)} %slice.29), channel_id=1, source_target_pairs={{0,4},{4,8},{8,12},{12,16},{16,20},{20,24},{24,28},{28,32},{32,36}... | collective-permute-start | bytes 12296 | tf_op jit(solution)/shard_map/ppermute | solution.py:55
  278.2 0.7 copy-start.5
Sparse Core Ops, SparseCore 0:
  20.5 41.5 all-gather.1
  278.4 37.3 reduce-scatter.1
where the time goes:
time: 328 us; the launch traced here: 326 us
  matrix products  127 us (39%)
  waiting for transfers between devices  84.7 us (26%)
  local copies, waits for them, and re-layouts  38.5 us (12%)
  other arithmetic  32.7 us (10%)
  starting transfers between devices  15.1 us (5%)
  between operations  13.7 us (4%)
  blocking collectives  13.4 us (4%)
    all_gather x1, waiting for transfers between devices, shards(): piece = lax.all_gather(normed_local, 'tp', axis=1, tiled=True)  41.5 us
    reduce_scatter x1, waiting for transfers between devices, shards(): lax.psum_scatter((jnp.dot(rec_out, recurrence_output_weight, preferred_el...  36.9 us
    dot_general x5, matrix products, shards(): jnp.dot(piece, weight, preferred_element_type=jnp.float32)  29.1 us
    dot_general x12, matrix products, block_pass(): jnp.einsum('bqy,byx->bqx', query_scaled_rows, latent_state, precision=PRE...  23.2 us
    dot_general x12, matrix products, block_pass(): jnp.einsum('otm,ote->ome', scaled_key * jnp.exp(block_total)[:, None, :],...  19.4 us
    dynamic_update_slice x12, other arithmetic, shards(): lax.scan(block_pass, (zero_state, zero_total), (to_blocks(query_rows, DK)...  19 us
    dot_general x12, matrix products, block_pass(): jnp.einsum('htk,hsk->hts', query_scaled_rows, scaled_key, precision=PRECI...  15.9 us
    dot_general x12, matrix products, block_pass(): jnp.einsum('hts,hsv->htv', scores, value_rows, precision=PRECISE_PRODUCT)  14 us
  transfers between devices with their start and end apart: 5, of which 3 were waited for; matrix products, arithmetic and copies ran while one was open for 9% of the time, Pallas kernels for 0%

commit v1 on v0

v1 whole, which is shorter than its diff:
```python
import jax
import jax.numpy as jnp
from jax import lax
from jax.experimental import pallas as pl
from jax.experimental.pallas import tpu as pltpu
from jax.sharding import PartitionSpec as P

DK = 128
DV = 128
BLK = 64
EPS = 1e-06
MESH = pl.DeviceIdType.MESH
F32 = jnp.float32
BF16 = jnp.bfloat16
VMEM_LIMIT = 62 * 1024 * 1024

NT = (((1,), (1,)), ((), ()))
TN = (((0,), (0,)), ((), ()))


def dot(a, b, dims=None):
    if dims is None:
        return jnp.dot(a, b, preferred_element_type=F32)
    return lax.dot_general(a, b, dims, preferred_element_type=F32)


def sigmoid(v):
    return 1.0 / (1.0 + jnp.exp(-v))


def log_one_minus(u):
    return -u * (1.0 + u * (1 / 2 + u * (1 / 3 + u * (1 / 4 + u * (1 / 5 + u * (1 / 6))))))


def greet(axis, peers):
    barrier = pltpu.get_barrier_semaphore()
    for peer in peers:
        pl.semaphore_signal(barrier, inc=1, device_id={axis: peer}, device_id_type=MESH)
    pl.semaphore_wait(barrier, len(peers))


def gather_project(chunks, n_sp, *refs):
    x, gain, surge, fmin, taps = refs[:5]
    ws = refs[5:12]
    part, qs, og, cv, hd, rim, st = refs[12:19]
    (xl, xr, xo, xn, wv, sv, pr, mx, state, run, tri2, wsem, ssem) = refs[19:32]
    s_or, s_ol, s_fr, s_fl, r_l, r_r, r_oa, r_ob = refs[32:40]
    tokens, width = x.shape
    tc = tokens // chunks
    half = tc // 2
    heads = width // DK
    own_rows = DK // n_sp
    me = lax.axis_index("tp")
    right, left, opp = lax.rem(me + 1, 4), lax.rem(me + 3, 4), lax.rem(me + 2, 4)
    srcs = (me, left, right, opp)

    loads = []
    for k in range(len(ws)):
        for r in range(4):
            rows = pl.ds(pl.multiple_of(srcs[r] * width, width), width)
            loads.append(
                pltpu.make_async_copy(
                    ws[k].at[rows, :], wv.at[k, pl.ds(r * width, width), :], wsem.at[k, r]
                )
            )
    for copy in loads:
        copy.start()
    surge_load = pltpu.make_async_copy(surge, sv, ssem)
    surge_load.start()

    greet("tp", (left, right))

    def rows_of(c, size, off=0):
        return pl.ds(pl.multiple_of(c * tc + off, 16), size)

    def own(c, to_right):
        rows = rows_of(c, tc)
        return pltpu.make_async_remote_copy(
            src_ref=x.at[rows, :],
            dst_ref=(xl if to_right else xr).at[rows, :],
            send_sem=(s_or if to_right else s_ol).at[c],
            recv_sem=(r_l if to_right else r_r).at[c],
            device_id={"tp": right if to_right else left},
            device_id_type=MESH,
        )

    def forward(c, to_right):
        rows = rows_of(c, half, 0 if to_right else half)
        return pltpu.make_async_remote_copy(
            src_ref=(xl if to_right else xr).at[rows, :],
            dst_ref=xo.at[rows, :],
            send_sem=(s_fr if to_right else s_fl).at[c],
            recv_sem=(r_oa if to_right else r_ob).at[c],
            device_id={"tp": right if to_right else left},
            device_id_type=MESH,
        )

    def pass_on(c):
        own(c, True).wait_recv()
        forward(c, True).start()
        own(c, False).wait_recv()
        forward(c, False).start()

    lead = min(2, chunks)
    for c in range(lead):
        own(c, True).start()
        own(c, False).start()

    state[...] = jnp.zeros_like(state)
    run[...] = jnp.zeros_like(run)
    mx[...] = jnp.zeros_like(mx)
    row = lax.broadcasted_iota(jnp.int32, (BLK, 2 * BLK), 0)
    col = lax.broadcasted_iota(jnp.int32, (BLK, 2 * BLK), 1)
    tri2[...] = jnp.where(row >= lax.rem(col, BLK), 1.0, 0.0).astype(BF16)

    pass_on(0)
    if chunks > lead:
        own(lead, True).start()
        own(lead, False).start()
    for copy in loads:
        copy.wait()
    surge_load.wait()

    def chunk(c, carry):
        @pl.when(c + 1 < chunks)
        def _():
            pass_on(c + 1)

        @pl.when(c + 1 + lead < chunks)
        def _():
            own(c + 1 + lead, True).start()
            own(c + 1 + lead, False).start()

        forward(c, True).wait_recv()
        forward(c, False).wait_recv()

        rows = rows_of(c, tc)
        total = jnp.zeros((tc, 1), F32)
        for piece in (x, xl, xr, xo):
            v = piece[rows, :].astype(F32)
            total = total + jnp.sum(v * v, axis=1, keepdims=True)
        scale = lax.rsqrt(total * (1.0 / (4 * width)) + EPS)
        for r, piece in enumerate((x, xl, xr, xo)):
            g = gain[srcs[r]].astype(F32)
            v = piece[rows, :].astype(F32) * scale * g
            xn[:, r * width : (r + 1) * width] = v.astype(BF16)

        def project(k, carry):
            pr[k] = dot(xn[...], wv[k]).astype(BF16)
            return carry

        lax.fori_loop(0, len(ws), project, 0)

        for b in range(tc // BLK):
            lr = slice(b * BLK, (b + 1) * BLK)
            gr = rows_of(c, BLK, b * BLK)
            for h in range(heads):
                ln = slice(h * DK, (h + 1) * DK)
                u = (1.0 - fmin[:, ln]) * sigmoid(-pr[1, lr, ln].astype(F32))
                lg = log_one_minus(u) + sv[gr, ln]
                hi = lg.astype(BF16)
                lo = (lg - hi.astype(F32)).astype(BF16)
                cum = dot(tri2[...], jnp.concatenate([hi, lo], axis=0))
                ref = cum[BLK // 2 - 1 : BLK // 2, :]
                tot = cum[BLK - 1 : BLK, :]
                d = cum - ref
                qraw = pr[0, lr, ln].astype(F32)
                qt = qraw * sigmoid(qraw) * (DK**-0.5) * jnp.exp(d)
                kt = u * jnp.exp(-d)
                runh = run[:, ln]
                qc = (qt * jnp.exp(ref)).astype(BF16)
                qs[gr, ln] = (qt * jnp.exp(ref + runh)).astype(BF16)
                kh = (kt * jnp.exp(tot - ref)).astype(BF16)
                v = pr[2, lr, ln]
                sc = dot(qt.astype(BF16), kt.astype(BF16), NT)
                ri = lax.broadcasted_iota(jnp.int32, (BLK, BLK), 0)
                ci = lax.broadcasted_iota(jnp.int32, (BLK, BLK), 1)
                sc = jnp.where(ri >= ci, sc, 0.0).astype(BF16)
                sh = state[h]
                part[gr, ln] = dot(sc, v) + dot(qc, sh.astype(BF16), NT)
                state[h] = jnp.exp(tot) * sh + dot(v, kh, TN)
                run[:, ln] = runh + tot

        og[rows, :] = pr[3]
        mx[8:, :] = pr[5].astype(F32) * pr[6].astype(F32)
        t = taps[...].astype(F32)
        conv = mx[6 : 6 + tc, :] * t[0:1] + mx[7 : 7 + tc, :] * t[1:2] + mx[8:, :] * t[2:3]
        post = pr[4].astype(F32)
        cv[rows, :] = (post * conv).astype(BF16)

        @pl.when(c == 0)
        def _():
            hd[0:8, :] = conv[0:8]
            hd[8:16, :] = post[0:8]

        mx[0:8, :] = mx[tc : tc + 8, :]
        return carry

    lax.fori_loop(0, chunks, chunk, 0)

    rim[...] = mx[0:8, :]
    for h in range(heads):
        sh = state[h].T
        decay = jnp.exp(run[:, h * DK : (h + 1) * DK])
        for j in range(n_sp):
            st[j, h * own_rows : (h + 1) * own_rows, :] = sh[j * own_rows : (j + 1) * own_rows]
            st[j, heads * own_rows + h : heads * own_rows + h + 1, :] = decay

    def finish(c, carry):
        own(c, True).wait_send()
        own(c, False).wait_send()
        forward(c, True).wait_send()
        forward(c, False).wait_send()
        return carry

    lax.fori_loop(0, chunks, finish, 0)


def pass_states(n_sp, heads, *refs):
    st, start, rim, sin, rim_in = refs[:5]
    got, back, dcol, s1, r1, s2, r2, rs, rr = refs[5:]
    rows = start.shape[0] * start.shape[1]
    own_rows = start.shape[1]
    me = lax.axis_index("sp")
    barrier = pltpu.get_barrier_semaphore()

    def hello(d, carry):
        pl.semaphore_signal(
            barrier, inc=1, device_id={"sp": lax.rem(me + d, n_sp)}, device_id_type=MESH
        )
        return carry

    lax.fori_loop(1, n_sp, hello, 0)
    pl.semaphore_wait(barrier, n_sp - 1)

    def there(d):
        to = lax.rem(me + d, n_sp)
        return pltpu.make_async_remote_copy(
            src_ref=st.at[to],
            dst_ref=got.at[me],
            send_sem=s1.at[d],
            recv_sem=r1.at[d],
            device_id={"sp": to},
            device_id_type=MESH,
        )

    def again(d):
        to = lax.rem(me + d, n_sp)
        return pltpu.make_async_remote_copy(
            src_ref=back.at[to],
            dst_ref=sin.at[me],
            send_sem=s2.at[d],
            recv_sem=r2.at[d],
            device_id={"sp": to},
            device_id_type=MESH,
        )

    def rim_copy():
        return pltpu.make_async_remote_copy(
            src_ref=rim,
            dst_ref=rim_in,
            send_sem=rs,
            recv_sem=rr,
            device_id={"sp": lax.rem(me + 1, n_sp)},
            device_id_type=MESH,
        )

    def each(f):
        def step(d, carry):
            f(d)
            return carry

        lax.fori_loop(1, n_sp, step, 0)

    each(lambda d: there(d).start())
    rim_copy().start()
    got[me] = st[me]
    each(lambda d: there(d).wait_recv())

    hrow = lax.broadcasted_iota(jnp.int32, (rows, DK), 0)
    lane = lax.broadcasted_iota(jnp.int32, (rows, DK), 1)
    pick = lane == me * own_rows + lax.rem(hrow, own_rows)
    for j in range(n_sp):
        dec = jnp.concatenate(
            [
                jnp.broadcast_to(got[j, rows + h : rows + h + 1, :], (own_rows, DK))
                for h in range(heads)
            ],
            axis=0,
        )
        one = jnp.sum(jnp.where(pick, dec, 0.0), axis=1, keepdims=True)
        dcol[j] = jnp.broadcast_to(one, (rows, DK))
    cur = jnp.concatenate([start[h] for h in range(heads)], axis=0)
    for j in range(n_sp):
        back[j] = cur
        cur = dcol[j] * cur + got[j, 0:rows, :]

    each(lambda d: again(d).start())
    sin[me] = back[me]
    each(lambda d: again(d).wait_recv())
    rim_copy().wait_recv()

    def drain(d):
        there(d).wait_send()
        again(d).wait_send()

    each(drain)
    rim_copy().wait_send()


def merge_scatter(n_sp, *refs):
    part, qs, og, cv, hd, rim_in, sin, taps, hgain, wr, wc, ogain, out = refs[:13]
    sb, rec, cvo, po, pp, ra, rb, fl, fr, acc, s_a, s_b, r_a, r_b, s_r, s_l, r_fl, r_fr = refs[13:]
    tokens, width = part.shape
    heads = width // DK
    own_rows = DK // n_sp
    me = lax.axis_index("tp")
    sp = lax.axis_index("sp")
    right, left, opp = lax.rem(me + 1, 4), lax.rem(me + 3, 4), lax.rem(me + 2, 4)
    tb = tokens // 4
    cols = wr.shape[1] // 2

    greet("tp", (left, right))

    for h in range(heads):
        for i in range(n_sp):
            sb[h, i * own_rows : (i + 1) * own_rows, :] = sin[
                i, h * own_rows : (h + 1) * own_rows, :
            ]

    t = taps[...].astype(F32)
    inside = jnp.where(sp == 0, 0.0, 1.0)
    e0 = rim_in[6:7, :] * inside
    e1 = rim_in[7:8, :] * inside
    add0 = e0 * t[0:1] + e1 * t[1:2]
    add1 = e1 * t[0:1]
    ri = lax.broadcasted_iota(jnp.int32, (8, width), 0)
    fix = jnp.where(ri == 0, add0, jnp.where(ri == 1, add1, 0.0))
    head = hd[8:16, :] * (hd[0:8, :] + fix)
    cvo[...] = cv[...]
    cvo[0:16, :] = jnp.concatenate([head, cv[8:16, :].astype(F32)], axis=0).astype(BF16)

    hg = hgain[...].astype(F32)

    def block_rows(owner):
        return pl.ds(pl.multiple_of(owner * tb, 16), tb)

    def mix_heads(owner):
        rows = block_rows(owner)
        for h in range(heads):
            ln = slice(h * DK, (h + 1) * DK)
            o = part[rows, ln] + dot(qs[rows, ln], sb[h].astype(BF16))
            o = o * lax.rsqrt(jnp.mean(o * o, axis=-1, keepdims=True) + EPS) * hg
            g = og[rows, ln].astype(F32)
            rec[rows, ln] = (o * (g * sigmoid(g))).astype(BF16)

    step = 512 if cols % 512 == 0 else cols

    def product(owner, side, put):
        rows = block_rows(owner)

        def one(n, carry):
            cs = pl.ds(pl.multiple_of(n * step, step), step)
            ws = pl.ds(pl.multiple_of(side * cols + n * step, step), step)
            put(cs, dot(rec[rows, :], wr[:, ws]) + dot(cvo[rows, :], wc[:, ws]))
            return carry

        lax.fori_loop(0, cols // step, one, 0)

    def remote(src, dst, ss, rs, to_right):
        return pltpu.make_async_remote_copy(
            src_ref=src,
            dst_ref=dst,
            send_sem=ss,
            recv_sem=rs,
            device_id={"tp": right if to_right else left},
            device_id_type=MESH,
        )

    far_a = remote(po.at[0], ra, s_a, r_a, True)
    far_b = remote(po.at[1], rb, s_b, r_b, False)
    near_r = [remote(pp.at[0, s], fl.at[s], s_r.at[s], r_fl.at[s], True) for s in range(2)]
    near_l = [remote(pp.at[1, s], fr.at[s], s_l.at[s], r_fr.at[s], False) for s in range(2)]

    def store(ref):
        def put(cs, v):
            ref[:, cs] = v.astype(BF16)

        return put

    def store_sum(ref, other):
        def put(cs, v):
            ref[:, cs] = (v + other[:, cs].astype(F32)).astype(BF16)

        return put

    mix_heads(opp)
    product(opp, 0, store(po.at[0]))
    far_a.start()
    product(opp, 1, store(po.at[1]))
    far_b.start()
    mix_heads(right)
    product(right, 1, store(pp.at[0, 1]))
    near_r[1].start()
    mix_heads(left)
    product(left, 0, store(pp.at[1, 0]))
    near_l[0].start()
    mix_heads(me)
    for side in range(2):
        product(me, side, lambda cs, v, side=side: acc.at[side].__setitem__((slice(None), cs), v))
    far_a.wait_recv()
    product(right, 0, store_sum(pp.at[0, 0], ra))
    near_r[0].start()
    far_b.wait_recv()
    product(left, 1, store_sum(pp.at[1, 1], rb))
    near_l[1].start()

    sq = jnp.zeros((tb, 1), F32)
    for side in (1, 0):
        near_r[side].wait_recv()
        near_l[side].wait_recv()
        for n in range(cols // step):
            cs = slice(n * step, (n + 1) * step)
            v = acc[side, :, cs] + fl[side, :, cs].astype(F32) + fr[side, :, cs].astype(F32)
            acc[side, :, cs] = v
            sq = sq + jnp.sum(v * v, axis=1, keepdims=True)
    scale = lax.rsqrt(sq * (1.0 / (2 * cols)) + EPS)
    for side in range(2):
        for n in range(cols // step):
            cs = slice(n * step, (n + 1) * step)
            gs = slice(side * cols + n * step, side * cols + (n + 1) * step)
            out[:, gs] = (acc[side, :, cs] * scale * ogain[:, gs].astype(F32)).astype(BF16)
    far_a.wait_send()
    far_b.wait_send()
    for s in range(2):
        near_r[s].wait_send()
        near_l[s].wait_send()


def solution(mesh):
    n_sp = mesh.shape["sp"]
    vm = pl.BlockSpec(memory_space=pltpu.VMEM)
    hbm = pl.BlockSpec(memory_space=pl.ANY)
    dma = pltpu.SemaphoreType.DMA
    chunks = 4

    def params(cid):
        return pltpu.CompilerParams(
            collective_id=cid, has_side_effects=True, vmem_limit_bytes=VMEM_LIMIT
        )

    def body(x, ing, wq, wf, wval, wog, wpost, wpre, wcv, fmin, surge, taps, hgain, start, wr, wc, ong):
        tokens, width = x.shape
        tc = tokens // chunks
        heads = width // DK
        own_rows = DK // n_sp
        rows = heads * own_rows
        mrows = rows + 8
        sds = jax.ShapeDtypeStruct
        part, qs, og, cv, hd, rim, st = pl.pallas_call(
            lambda *refs: gather_project(chunks, n_sp, *refs),
            out_shape=(
                sds((tokens, width), F32),
                sds((tokens, width), BF16),
                sds((tokens, width), BF16),
                sds((tokens, width), BF16),
                sds((16, width), F32),
                sds((8, width), F32),
                sds((n_sp, mrows, DK), F32),
            ),
            in_specs=[vm, vm, hbm, vm, vm] + [hbm] * 7,
            out_specs=(vm,) * 7,
            scratch_shapes=[
                pltpu.VMEM((tokens, width), BF16),
                pltpu.VMEM((tokens, width), BF16),
                pltpu.VMEM((tokens, width), BF16),
                pltpu.VMEM((tc, 4 * width), BF16),
                pltpu.VMEM((7, 4 * width, width), BF16),
                pltpu.VMEM((tokens, width), F32),
                pltpu.VMEM((7, tc, width), BF16),
                pltpu.VMEM((tc + 8, width), F32),
                pltpu.VMEM((heads, DV, DK), F32),
                pltpu.VMEM((1, width), F32),
                pltpu.VMEM((BLK, 2 * BLK), BF16),
                dma((7, 4)),
                dma,
            ]
            + [dma((chunks,))] * 8,
            compiler_params=params(0),
            name="gather_project",
        )(x, ing.reshape(4, 1, width), surge, fmin.reshape(1, width), taps, wq, wf, wval, wog, wpost, wpre, wcv)

        sin, rim_in = pl.pallas_call(
            lambda *refs: pass_states(n_sp, heads, *refs),
            out_shape=(sds((n_sp, rows, DK), F32), sds((8, width), F32)),
            in_specs=[vm] * 3,
            out_specs=(vm, vm),
            scratch_shapes=[
                pltpu.VMEM((n_sp, mrows, DK), F32),
                pltpu.VMEM((n_sp, rows, DK), F32),
                pltpu.VMEM((n_sp, rows, DK), F32),
            ]
            + [dma((n_sp,))] * 4
            + [dma, dma],
            compiler_params=params(1),
            name="pass_states",
        )(st, start, rim)

        tb = tokens // 4
        cols = wr.shape[1] // 2
        return pl.pallas_call(
            lambda *refs: merge_scatter(n_sp, *refs),
            out_shape=sds((tb, 2 * cols), BF16),
            in_specs=[vm] * 12,
            out_specs=vm,
            scratch_shapes=[
                pltpu.VMEM((heads, DK, DV), F32),
                pltpu.VMEM((tokens, width), BF16),
                pltpu.VMEM((tokens, width), BF16),
                pltpu.VMEM((2, tb, cols), BF16),
                pltpu.VMEM((2, 2, tb, cols), BF16),
                pltpu.VMEM((tb, cols), BF16),
                pltpu.VMEM((tb, cols), BF16),
                pltpu.VMEM((2, tb, cols), BF16),
                pltpu.VMEM((2, tb, cols), BF16),
                pltpu.VMEM((2, tb, cols), F32),
                dma, dma, dma, dma,
                dma((2,)), dma((2,)), dma((2,)), dma((2,)),
            ],
            compiler_params=params(2),
            name="merge_scatter",
        )(part, qs, og, cv, hd, rim_in, sin, taps, hgain.reshape(1, DV), wr, wc, ong.reshape(1, 2 * cols))

    in_specs = (
        P("sp", "tp"),
        P(),
        P(None, "tp"),
        P(None, "tp"),
        P(None, "tp"),
        P(None, "tp"),
        P(None, "tp"),
        P(None, "tp"),
        P(None, "tp"),
        P("tp"),
        P("sp", "tp"),
        P(None, "tp"),
        P(),
        P("tp", "sp", None),
        P("tp", None),
        P("tp", None),
        P(),
    )
    return jax.shard_map(
        body, mesh=mesh, in_specs=in_specs, out_specs=P(("sp", "tp"), None), check_vma=False
    )
```

time: 328 us -> 112 us (0.34)
  matrix products: 127 us -> 0 us
  Pallas kernels: 0 us -> 107 us
  waiting for transfers between devices: 84.7 us -> 0 us
  local copies, waits for them, and re-layouts: 38.5 us -> 4.67 us
  other arithmetic: 32.7 us -> 0 us
  starting transfers between devices: 15.1 us -> 0 us
  between operations: 13.7 us -> 0.03 us
  blocking collectives: 13.4 us -> 0 us
    dot_general x56 -> x0, matrix products: 127 us -> none  [the longest x5 29.1 us: shards(): jnp.dot(piece, weight, preferred_element_type=jnp.float32)]
    pallas_call x0 -> x3, Pallas kernels: none -> 107 us  [the longest x1 46.8 us: body(): pl.pallas_call(lambda *refs: gather_project(chunks, n_sp, *refs), out_sha...]
    all_gather x1 -> x0, waiting for transfers between devices: 41.5 us -> none  [shards(): piece = lax.all_gather(normed_local, 'tp', axis=1, tiled=True)]
    reduce_scatter x1 -> x0, waiting for transfers between devices: 36.9 us -> none  [shards(): lax.psum_scatter((jnp.dot(rec_out, recurrence_output_weight, preferred_el...]
    dynamic_update_slice x12 -> x0, other arithmetic: 19 us -> none  [shards(): lax.scan(block_pass, (zero_state, zero_total), (to_blocks(query_rows, DK)...]
    transpose x4 -> x0, local copies, waits for them, and re-layouts: 12.6 us -> none  [the longest x3 8.98 us: to_blocks(): value_rows.reshape(blocks, BLK, heads_local, width).transpose(0, 2, 1, 3)]
    all_to_all x2 -> x0, starting transfers between devices: 11.4 us -> none  [the longest x1 7.89 us: in_one_piece(): lax.all_to_all(both, axis, split_axis=split_dim, concat_axis=concat_dim,...]
    squeeze x12 -> x0, local copies, waits for them, and re-layouts: 11 us -> none  [shards(): lax.scan(block_pass, (zero_state, zero_total), (to_blocks(query_rows, DK)...]
  transfers between devices with their start and end apart: 5 -> 0, of which waited for: 3 -> 0; matrix products, arithmetic and copies ran while one was open for 9% -> 0% of each run, Pallas kernels for 0% -> 0%
where the time goes in v1:
time: 112 us
  Pallas kernels  107 us (96%)
  local copies, waits for them, and re-layouts  4.67 us (4%)
    pallas_call x1, Pallas kernels, body(): pl.pallas_call(lambda *refs: gather_project(chunks, n_sp, *refs), out_sha...  46.8 us
    pallas_call x1, Pallas kernels, body(): pl.pallas_call(lambda *refs: merge_scatter(n_sp, *refs), out_shape=sds((t...  34.5 us
    pallas_call x1, Pallas kernels, body(): pl.pallas_call(lambda *refs: pass_states(n_sp, heads, *refs), out_shape=(...  25.5 us

profile of v1, /device:TPU:1, one launch (start us, length us, event | category | flops | bytes accessed | tf_op | source)
XLA Modules:
  0.0 111.5 jit_solution(13487150881573916487)
XLA Ops:
  0.0 1.3 %reshape.16.refs_1_ = bf16[4,1,512]{2,1,0:T(2,128)(2,1)} reshape(bf16[2048]{0:T(1024)(128)(2,1)} %param.18) | data formatting | bytes 8192 | tf_op jit(solution)/shard_map/reshape | solution.py:491
  1.3 1.3 %reshape.15.refs_11_ = bf16[1,2048]{1,0:T(2,128)(2,1)} reshape(bf16[2048]{0:T(1024)(128)(2,1)} %param.33) | data formatting | bytes 8192 | tf_op jit(solution)/shard_map/reshape | solution.py:532
  2.6 46.8 %gather_project.1 = (f32[768,512]{1,0:T(8,128)}, bf16[768,512]{1,0:T(8,128)(2,1)}, bf16[768,512]{1,0:T(8,128)(2,1)}, bf16[768,512]{1,0:T(8,128)(2,1)}, f32[16,51...) custom-call(bf16[768,512]{1,0:T(8,128)(2,1)} %refs_0_.1, bf16[4,1,512]{2,1,0:T(2,128)(2,1)} %reshape.16.refs_1_, ...), custom_call_target="tpu_custom_call" | custom-call | tf_op jit(solution)/shard_map/gather_project/pallas_call | solution.py:460
  49.4 25.5 %pass_states.1 = (f32[32,16,128]{2,1,0:T(8,128)}, f32[8,512]{1,0:T(8,128)}) custom-call(f32[32,24,128]{2,1,0:T(8,128)} %get-tuple-element.19.refs_0_, f32[4,4,128]{2,1,0:T(4,128)} %refs_1_.1, f32[8,512]{1,0:T(8,128)} %get-tuple-element.20.refs_2_), custom_call_target="tpu_custom_call" | custom-call | tf_op jit(solution)/shard_map/pass_states/pallas_call | solution.py:493
  74.9 34.5 %merge_scatter.1 = bf16[192,2048]{1,0:T(8,128)(2,1)} custom-call(f32[768,512]{1,0:T(8,128)} %get-tuple-element.14.refs_0_, bf16[768,512]{1,0:T(8,128)(2,1)} %get-tuple-element.15.refs_1_, bf16[768,512]{1,0:T(8,128)(2,1)} %get-tuple-element.16.refs_2_, bf16[768,512]{1,0:T(8,128)(2,1)} %get-tuple-element.17.refs_3_, f32[16,512]{1,0:T(8,128)} %get-tuple-element.18.refs_4_, ...), custom_call_target="tpu_custom_call" | custom-call | tf_op jit(solution)/shard_map/merge_scatter/pallas_call | solution.py:511
  109.4 2.1 %copy.20 = bf16[192,2048]{1,0:T(8,128)(2,1)} copy(bf16[192,2048]{1,0:T(8,128)(2,1)} %merge_scatter.1) | data formatting | bytes 1572864

commit v2 on v1

v2 whole, which is shorter than its diff:
```python
import jax
import jax.numpy as jnp
from jax import lax
from jax.experimental import pallas as pl
from jax.experimental.pallas import tpu as pltpu
from jax.sharding import PartitionSpec as P

DK = 128
DV = 128
BLK = 64
EPS = 1e-06
MESH = pl.DeviceIdType.MESH
F32 = jnp.float32
BF16 = jnp.bfloat16
VMEM_LIMIT = 62 * 1024 * 1024

NT = (((1,), (1,)), ((), ()))
TN = (((0,), (0,)), ((), ()))


def dot(a, b, dims=None):
    if dims is None:
        return jnp.dot(a, b, preferred_element_type=F32)
    return lax.dot_general(a, b, dims, preferred_element_type=F32)


def sigmoid(v):
    return 1.0 / (1.0 + jnp.exp(-v))


def log_one_minus(u):
    return -u * (1.0 + u * (1 / 2 + u * (1 / 3 + u * (1 / 4 + u * (1 / 5 + u * (1 / 6))))))


def layer(chunks, n_sp, *refs):
    x, gain, surge, fmin, taps, hgain, start, ogain = refs[:8]
    ws = refs[8:15]
    wr_in, wc_in, out = refs[15:18]
    (xl, xr, xo, xn, wv, wr, wc, sv, pr, pd, mx, state, run, tri2, gains) = refs[18:33]
    (part, qs, stf, st, got, dcol, back, sin, rim, rim_in, sb, rec, cvo, accc) = refs[33:47]
    (po, pp, ra, rb, fl, fr, acc) = refs[47:54]
    wsem, msem, s_or, s_ol, s_fr, s_fl, r_l, r_r, r_oa, r_ob = refs[54:64]
    s1, r1, s2, r2, rs, rr = refs[64:70]
    s_a, s_b, r_a, r_b, s_r, s_l, r_fl, r_fr = refs[70:]
    tokens, width = x.shape
    full = 4 * width
    tc = tokens // chunks
    half = tc // 2
    heads = width // DK
    own_rows = DK // n_sp
    srows = heads * own_rows
    tb = tokens // 4
    cols = full // 2
    me = lax.axis_index("tp")
    sp = lax.axis_index("sp")
    right, left, opp = lax.rem(me + 1, 4), lax.rem(me + 3, 4), lax.rem(me + 2, 4)
    srcs = (me, left, right, opp)

    first, later = [], []
    for k in range(7):
        for r in range(4):
            rows = pl.ds(pl.multiple_of(srcs[r] * width, width), width)
            copy = pltpu.make_async_copy(
                ws[k].at[rows, :], wv.at[k, pl.ds(r * width, width), :], wsem.at[k, r]
            )
            (first if k < 3 else later).append(copy)
    first.append(pltpu.make_async_copy(surge, sv, msem.at[0]))
    later.append(pltpu.make_async_copy(wr_in, wr, msem.at[1]))
    later.append(pltpu.make_async_copy(wc_in, wc, msem.at[2]))
    for copy in first + later:
        copy.start()

    barrier = pltpu.get_barrier_semaphore()
    for peer in (left, right):
        pl.semaphore_signal(barrier, inc=1, device_id={"tp": peer}, device_id_type=MESH)

    def each(f):
        def step(d, carry):
            f(d)
            return carry

        lax.fori_loop(1, n_sp, step, 0)

    each(
        lambda d: pl.semaphore_signal(
            barrier, inc=1, device_id={"sp": lax.rem(sp + d, n_sp)}, device_id_type=MESH
        )
    )
    pl.semaphore_wait(barrier, 2 + n_sp - 1)

    def beside(src, dst, ss, rs, to_right):
        return pltpu.make_async_remote_copy(
            src_ref=src,
            dst_ref=dst,
            send_sem=ss,
            recv_sem=rs,
            device_id={"tp": right if to_right else left},
            device_id_type=MESH,
        )

    def along(src, dst, ss, rs, to):
        return pltpu.make_async_remote_copy(
            src_ref=src,
            dst_ref=dst,
            send_sem=ss,
            recv_sem=rs,
            device_id={"sp": to},
            device_id_type=MESH,
        )

    def rows_of(c, size, off=0):
        return pl.ds(pl.multiple_of(c * tc + off, 16), size)

    def own(c, to_right):
        rows = rows_of(c, tc)
        return beside(
            x.at[rows, :],
            (xl if to_right else xr).at[rows, :],
            (s_or if to_right else s_ol).at[c],
            (r_l if to_right else r_r).at[c],
            to_right,
        )

    def forward(c, to_right):
        rows = rows_of(c, half, 0 if to_right else half)
        return beside(
            (xl if to_right else xr).at[rows, :],
            xo.at[rows, :],
            (s_fr if to_right else s_fl).at[c],
            (r_oa if to_right else r_ob).at[c],
            to_right,
        )

    def pass_on(c):
        own(c, True).wait_recv()
        forward(c, True).start()
        own(c, False).wait_recv()
        forward(c, False).start()

    lead = min(2, chunks)
    for c in range(lead):
        own(c, True).start()
        own(c, False).start()

    state[...] = jnp.zeros_like(state)
    run[...] = jnp.zeros_like(run)
    gains[...] = gain[...].astype(F32).reshape(1, full)
    row = lax.broadcasted_iota(jnp.int32, (BLK, 2 * BLK), 0)
    col = lax.broadcasted_iota(jnp.int32, (BLK, 2 * BLK), 1)
    tri2[...] = jnp.where(row >= lax.rem(col, BLK), 1.0, 0.0).astype(BF16)

    pass_on(0)
    if chunks > lead:
        own(lead, True).start()
        own(lead, False).start()
    for copy in first:
        copy.wait()

    def chunk(c, carry):
        @pl.when(c + 1 < chunks)
        def _():
            pass_on(c + 1)

        @pl.when(c + 1 + lead < chunks)
        def _():
            own(c + 1 + lead, True).start()
            own(c + 1 + lead, False).start()

        forward(c, True).wait_recv()
        forward(c, False).wait_recv()

        rows = rows_of(c, tc)
        total = jnp.zeros((tc, 1), F32)
        for piece in (x, xl, xr, xo):
            v = piece[rows, :].astype(F32)
            total = total + jnp.sum(v * v, axis=1, keepdims=True)
        scale = lax.rsqrt(total * (1.0 / full) + EPS)
        for r, piece in enumerate((x, xl, xr, xo)):
            g = gains[:, pl.ds(pl.multiple_of(srcs[r] * width, width), width)]
            v = piece[rows, :].astype(F32) * scale * g
            xn[rows, r * width : (r + 1) * width] = v.astype(BF16)

        def project(k, carry):
            pr[k] = dot(xn[rows, :], wv[k]).astype(BF16)
            return carry

        lax.fori_loop(0, 3, project, 0)

        for b in range(tc // BLK):
            lr = slice(b * BLK, (b + 1) * BLK)
            gr = rows_of(c, BLK, b * BLK)
            for h in range(heads):
                ln = slice(h * DK, (h + 1) * DK)
                u = (1.0 - fmin[:, ln]) * sigmoid(-pr[1, lr, ln].astype(F32))
                lg = log_one_minus(u) + sv[gr, ln]
                hi = lg.astype(BF16)
                lo = (lg - hi.astype(F32)).astype(BF16)
                cum = dot(tri2[...], jnp.concatenate([hi, lo], axis=0))
                ref = cum[BLK // 2 - 1 : BLK // 2, :]
                tot = cum[BLK - 1 : BLK, :]
                d = cum - ref
                qraw = pr[0, lr, ln].astype(F32)
                qt = qraw * sigmoid(qraw) * (DK**-0.5) * jnp.exp(d)
                kt = u * jnp.exp(-d)
                runh = run[:, ln]
                qc = (qt * jnp.exp(ref)).astype(BF16)
                qs[gr, ln] = (qt * jnp.exp(ref + runh)).astype(BF16)
                kh = (kt * jnp.exp(tot - ref)).astype(BF16)
                v = pr[2, lr, ln]
                sc = dot(qt.astype(BF16), kt.astype(BF16), NT)
                ri = lax.broadcasted_iota(jnp.int32, (BLK, BLK), 0)
                ci = lax.broadcasted_iota(jnp.int32, (BLK, BLK), 1)
                sc = jnp.where(ri >= ci, sc, 0.0).astype(BF16)
                sh = state[h]
                part[gr, ln] = dot(sc, v) + dot(qc, sh.astype(BF16), NT)
                state[h] = jnp.exp(tot) * sh + dot(v, kh, TN)
                run[:, ln] = runh + tot
        return carry

    lax.fori_loop(0, chunks, chunk, 0)

    for h in range(heads):
        sh = state[h].T
        decay = jnp.exp(run[:, h * DK : (h + 1) * DK])
        top = decay.astype(BF16).astype(F32)
        for j in range(n_sp):
            stf[j, h * own_rows : (h + 1) * own_rows, :] = sh[j * own_rows : (j + 1) * own_rows]
            stf[j, srows + h : srows + h + 1, :] = top
            stf[j, srows + heads + h : srows + heads + h + 1, :] = decay - top
    for j in range(n_sp):
        st[j] = stf[j].astype(BF16)

    def there(d):
        to = lax.rem(sp + d, n_sp)
        return along(st.at[to], got.at[sp], s1.at[d], r1.at[d], to)

    def again(d):
        to = lax.rem(sp + d, n_sp)
        return along(back.at[to], sin.at[sp], s2.at[d], r2.at[d], to)

    def rim_copy():
        return along(rim, rim_in, rs, rr, lax.rem(sp + 1, n_sp))

    each(lambda d: there(d).start())
    got[sp] = st[sp]

    for copy in later:
        copy.wait()

    def wide(k, carry):
        pd[k] = dot(xn[...], wv[k + 3]).astype(BF16)
        return carry

    lax.fori_loop(0, 2, wide, 0)
    mx[0:8, :] = jnp.zeros((8, width), F32)
    piece = tokens // 8

    def mixing(i, carry):
        rows = pl.ds(pl.multiple_of(i * piece, 16), piece)
        mx[pl.ds(pl.multiple_of(i * piece + 8, 8), piece), :] = pd[0, rows, :].astype(F32) * pd[
            1, rows, :
        ].astype(F32)
        return carry

    lax.fori_loop(0, 8, mixing, 0)
    rim[...] = mx[tokens : tokens + 8, :]
    rim_copy().start()

    each(lambda d: there(d).wait_recv())
    hrow = lax.broadcasted_iota(jnp.int32, (srows, DK), 0)
    lane = lax.broadcasted_iota(jnp.int32, (srows, DK), 1)
    pick = lane == sp * own_rows + lax.rem(hrow, own_rows)
    for j in range(n_sp):
        gj = got[j].astype(F32)
        both = gj[srows : srows + heads] + gj[srows + heads : srows + 2 * heads]
        dec = jnp.concatenate(
            [jnp.broadcast_to(both[h : h + 1, :], (own_rows, DK)) for h in range(heads)],
            axis=0,
        )
        one = jnp.sum(jnp.where(pick, dec, 0.0), axis=1, keepdims=True)
        dcol[j] = jnp.broadcast_to(one, (srows, DK))
    cur = jnp.concatenate([start[h] for h in range(heads)], axis=0)
    for j in range(n_sp):
        back[j] = cur.astype(BF16)
        cur = dcol[j] * cur + got[j].astype(F32)[0:srows]

    each(lambda d: again(d).start())
    sin[sp] = back[sp]

    lax.fori_loop(2, 4, wide, 0)
    rim_copy().wait_recv()
    inside = jnp.where(sp == 0, 0.0, 1.0)
    mx[0:8, :] = rim_in[...] * inside
    t = taps[...].astype(F32)

    def convolve(i, carry):
        rows = pl.ds(pl.multiple_of(i * piece, 16), piece)
        v = mx[pl.ds(pl.multiple_of(i * piece, 8), piece + 8), :]
        conv = v[6 : 6 + piece] * t[0:1] + v[7 : 7 + piece] * t[1:2] + v[8:] * t[2:3]
        cvo[rows, :] = (pd[2, rows, :].astype(F32) * conv).astype(BF16)
        return carry

    lax.fori_loop(0, 8, convolve, 0)

    step = 512 if cols % 512 == 0 else cols

    def conv_part(n, carry):
        cs = pl.ds(pl.multiple_of(n * step, step), step)
        accc[:, cs] = dot(cvo[...], wc[:, cs])
        return carry

    lax.fori_loop(0, full // step, conv_part, 0)

    each(lambda d: again(d).wait_recv())
    for i in range(n_sp):
        si = sin[i].astype(F32)
        for h in range(heads):
            sb[h, i * own_rows : (i + 1) * own_rows, :] = si[h * own_rows : (h + 1) * own_rows, :]

    hg = hgain[...].astype(F32)

    def block_rows(owner):
        return pl.ds(pl.multiple_of(owner * tb, 16), tb)

    def mix_heads(owner):
        rows = block_rows(owner)
        for h in range(heads):
            ln = slice(h * DK, (h + 1) * DK)
            o = part[rows, ln] + dot(qs[rows, ln], sb[h].astype(BF16))
            o = o * lax.rsqrt(jnp.mean(o * o, axis=-1, keepdims=True) + EPS) * hg
            g = pd[3, rows, ln].astype(F32)
            rec[rows, ln] = (o * (g * sigmoid(g))).astype(BF16)

    def product(owner, side, put):
        rows = block_rows(owner)

        def one(n, carry):
            cs = pl.ds(pl.multiple_of(n * step, step), step)
            ns = pl.ds(pl.multiple_of(side * cols + n * step, step), step)
            put(cs, dot(rec[rows, :], wr[:, ns]) + accc[rows, ns])
            return carry

        lax.fori_loop(0, cols // step, one, 0)

    far_a = beside(po.at[0], ra, s_a, r_a, True)
    far_b = beside(po.at[1], rb, s_b, r_b, False)
    near_r = [beside(pp.at[0, s], fl.at[s], s_r.at[s], r_fl.at[s], True) for s in range(2)]
    near_l = [beside(pp.at[1, s], fr.at[s], s_l.at[s], r_fr.at[s], False) for s in range(2)]

    def store(ref):
        def put(cs, v):
            ref[:, cs] = v.astype(BF16)

        return put

    def store_sum(ref, other):
        def put(cs, v):
            ref[:, cs] = (v + other[:, cs].astype(F32)).astype(BF16)

        return put

    def keep(side):
        def put(cs, v):
            acc[side, :, cs] = v

        return put

    mix_heads(opp)
    product(opp, 0, store(po.at[0]))
    far_a.start()
    product(opp, 1, store(po.at[1]))
    far_b.start()
    mix_heads(right)
    product(right, 1, store(pp.at[0, 1]))
    near_r[1].start()
    mix_heads(left)
    product(left, 0, store(pp.at[1, 0]))
    near_l[0].start()
    mix_heads(me)
    for side in range(2):
        product(me, side, keep(side))
    far_a.wait_recv()
    product(right, 0, store_sum(pp.at[0, 0], ra))
    near_r[0].start()
    far_b.wait_recv()
    product(left, 1, store_sum(pp.at[1, 1], rb))
    near_l[1].start()

    sq = jnp.zeros((tb, 1), F32)
    for side in (1, 0):
        near_r[side].wait_recv()
        near_l[side].wait_recv()
        for n in range(cols // step):
            cs = slice(n * step, (n + 1) * step)
            v = acc[side, :, cs] + fl[side, :, cs].astype(F32) + fr[side, :, cs].astype(F32)
            acc[side, :, cs] = v
            sq = sq + jnp.sum(v * v, axis=1, keepdims=True)
    scale = lax.rsqrt(sq * (1.0 / full) + EPS)
    gains[...] = ogain[...].astype(F32).reshape(1, full)
    for side in range(2):
        for n in range(cols // step):
            cs = slice(n * step, (n + 1) * step)
            gs = slice(side * cols + n * step, side * cols + (n + 1) * step)
            out[:, gs] = (acc[side, :, cs] * scale * gains[:, gs]).astype(BF16)

    def finish(c, carry):
        own(c, True).wait_send()
        own(c, False).wait_send()
        forward(c, True).wait_send()
        forward(c, False).wait_send()
        return carry

    lax.fori_loop(0, chunks, finish, 0)

    def drain(d):
        there(d).wait_send()
        again(d).wait_send()

    each(drain)
    rim_copy().wait_send()
    far_a.wait_send()
    far_b.wait_send()
    for s in range(2):
        near_r[s].wait_send()
        near_l[s].wait_send()


def solution(mesh):
    n_sp = mesh.shape["sp"]
    vm = pl.BlockSpec(memory_space=pltpu.VMEM)
    hbm = pl.BlockSpec(memory_space=pl.ANY)
    dma = pltpu.SemaphoreType.DMA
    chunks = 4

    def body(x, ing, wq, wf, wval, wog, wpost, wpre, wcv, fmin, surge, taps, hgain, start, wr, wc, ong):
        tokens, width = x.shape
        tc = tokens // chunks
        heads = width // DK
        own_rows = DK // n_sp
        rows = heads * own_rows
        mrows = rows + 2 * heads
        tb = tokens // 4
        full = 4 * width
        cols = full // 2
        v = pltpu.VMEM
        return pl.pallas_call(
            lambda *refs: layer(chunks, n_sp, *refs),
            out_shape=jax.ShapeDtypeStruct((tb, full), BF16),
            in_specs=[vm, vm, hbm, vm, vm, vm, vm, vm] + [hbm] * 9,
            out_specs=vm,
            scratch_shapes=[
                v((tokens, width), BF16),
                v((tokens, width), BF16),
                v((tokens, width), BF16),
                v((tokens, full), BF16),
                v((7, full, width), BF16),
                v((width, full), BF16),
                v((width, full), BF16),
                v((tokens, width), F32),
                v((3, tc, width), BF16),
                v((4, tokens, width), BF16),
                v((tokens + 8, width), F32),
                v((heads, DV, DK), F32),
                v((1, width), F32),
                v((BLK, 2 * BLK), BF16),
                v((1, full), F32),
                v((tokens, width), F32),
                v((tokens, width), BF16),
                v((n_sp, mrows, DK), F32),
                v((n_sp, mrows, DK), BF16),
                v((n_sp, mrows, DK), BF16),
                v((n_sp, rows, DK), F32),
                v((n_sp, rows, DK), BF16),
                v((n_sp, rows, DK), BF16),
                v((8, width), F32),
                v((8, width), F32),
                v((heads, DK, DV), F32),
                v((tokens, width), BF16),
                v((tokens, width), BF16),
                v((tokens, full), F32),
                v((2, tb, cols), BF16),
                v((2, 2, tb, cols), BF16),
                v((tb, cols), BF16),
                v((tb, cols), BF16),
                v((2, tb, cols), BF16),
                v((2, tb, cols), BF16),
                v((2, tb, cols), F32),
                dma((7, 4)),
                dma((3,)),
            ]
            + [dma((chunks,))] * 8
            + [dma((n_sp,))] * 4
            + [dma] * 6
            + [dma((2,))] * 4,
            compiler_params=pltpu.CompilerParams(
                collective_id=0, has_side_effects=True, vmem_limit_bytes=VMEM_LIMIT
            ),
            name="layer",
        )(x, ing, surge, fmin.reshape(1, width), taps, hgain.reshape(1, DV), start, ong,
          wq, wf, wval, wpre, wcv, wpost, wog, wr, wc)

    in_specs = (
        P("sp", "tp"),
        P(),
        P(None, "tp"),
        P(None, "tp"),
        P(None, "tp"),
        P(None, "tp"),
        P(None, "tp"),
        P(None, "tp"),
        P(None, "tp"),
        P("tp"),
        P("sp", "tp"),
        P(None, "tp"),
        P(),
        P("tp", "sp", None),
        P("tp", None),
        P("tp", None),
        P(),
    )
    return jax.shard_map(
        body, mesh=mesh, in_specs=in_specs, out_specs=P(("sp", "tp"), None), check_vma=False
    )
```

time: 112 us -> 90.7 us (0.81)
  Pallas kernels: 107 us -> 88.4 us
  local copies, waits for them, and re-layouts: 4.67 us -> 2.09 us
    pallas_call x3 -> x1, Pallas kernels: 107 us -> 88.4 us  [body(): pl.pallas_call(lambda *refs: layer(chunks, n_sp, *refs), out_shape=jax.Sh...]
    reshape x2 -> x0, local copies, waits for them, and re-layouts: 2.58 us -> none  [the longest x1 1.29 us: body(): ing.reshape(4, 1, width)]
where the time goes in v2:
time: 90.7 us; the launch traced here: 90.5 us
  Pallas kernels  88.4 us (97%)
  local copies, waits for them, and re-layouts  2.09 us (2%)
    pallas_call x1, Pallas kernels, body(): pl.pallas_call(lambda *refs: layer(chunks, n_sp, *refs), out_shape=jax.Sh...  88.4 us
    unnamed x1, local copies, waits for them, and re-layouts  2.09 us

profile of v2, /device:TPU:1, one launch (start us, length us, event | category | flops | bytes accessed | tf_op | source)
XLA Modules:
  0.0 90.5 jit_solution(4602806141376415171)
XLA Ops:
  0.0 88.4 %layer.1 = bf16[192,2048]{1,0:T(8,128)(2,1)} custom-call(bf16[768,512]{1,0:T(8,128)(2,1)} %refs_0_.1, bf16[2048]{0:T(1024)(128)(2,1)} %refs_1_.1, f32[768,512]{1,0:T(8,128)} %refs_2_.1, f32[1,512]{1,0:T(1,128)} %bitcast.2, bf16[3,512]{1,0:T(4,128)(2,1)} %refs_4_.1, bf16[1,128]{1,0:T(2,128)(2,1)} %bitcast.3, f32[4,4,128]{2,1,0:T(4,128)} %refs_6_.1, ...), custom_call_target="tpu_custom_call" | custom-call | tf_op jit(solution)/shard_map/layer/pallas_call | solution.py:446
  88.4 2.1 %copy.19 = bf16[192,2048]{1,0:T(8,128)(2,1)} copy(bf16[192,2048]{1,0:T(8,128)(2,1)} %layer.1) | data formatting | bytes 1572864

commit v3 on v2

--- a/solution.py
+++ b/solution.py
@@ -25,7 +25,7 @@
 
 
 def sigmoid(v):
-    return 1.0 / (1.0 + jnp.exp(-v))
+    return lax.logistic(v)
 
 
 def log_one_minus(u):
@@ -37,15 +37,17 @@
     ws = refs[8:15]
     wr_in, wc_in, out = refs[15:18]
     (xl, xr, xo, xn, wv, wr, wc, sv, pr, pd, mx, state, run, tri2, gains) = refs[18:33]
-    (part, qs, stf, st, got, dcol, back, sin, rim, rim_in, sb, rec, cvo, accc) = refs[33:47]
-    (po, pp, ra, rb, fl, fr, acc) = refs[47:54]
-    wsem, msem, s_or, s_ol, s_fr, s_fl, r_l, r_r, r_oa, r_ob = refs[54:64]
-    s1, r1, s2, r2, rs, rr = refs[64:70]
-    s_a, s_b, r_a, r_b, s_r, s_l, r_fl, r_fr = refs[70:]
+    (part3, scales, part, qs, stf, st, got, dcol, back, sin, rim, rim_in, sb, rec, cvo, accc) = refs[33:49]
+    (po, pp, ra, rb, fl, fr, acc) = refs[49:56]
+    known, wsem, msem, s_or, s_ol, s_fr, s_fl, r_l, r_r, r_oa, r_ob = refs[56:67]
+    s1, r1, s2, r2, rs, rr = refs[67:73]
+    s_a, s_b, r_a, r_b, s_r, s_l, r_fl, r_fr = refs[73:]
     tokens, width = x.shape
     full = 4 * width
     tc = tokens // chunks
-    half = tc // 2
+    parts = 2 * chunks
+    tm = tokens // parts
+    half = tm // 2
     heads = width // DK
     own_rows = DK // n_sp
     srows = heads * own_rows
@@ -56,18 +58,18 @@
     right, left, opp = lax.rem(me + 1, 4), lax.rem(me + 3, 4), lax.rem(me + 2, 4)
     srcs = (me, left, right, opp)
 
-    first, later = [], []
+    first, early, later = [], [], []
     for k in range(7):
         for r in range(4):
             rows = pl.ds(pl.multiple_of(srcs[r] * width, width), width)
             copy = pltpu.make_async_copy(
                 ws[k].at[rows, :], wv.at[k, pl.ds(r * width, width), :], wsem.at[k, r]
             )
-            (first if k < 3 else later).append(copy)
+            (early if r == 0 else first if k < 3 else later).append(copy)
     first.append(pltpu.make_async_copy(surge, sv, msem.at[0]))
     later.append(pltpu.make_async_copy(wr_in, wr, msem.at[1]))
     later.append(pltpu.make_async_copy(wc_in, wc, msem.at[2]))
-    for copy in first + later:
+    for copy in early + first + later:
         copy.start()
 
     barrier = pltpu.get_barrier_semaphore()
@@ -81,12 +83,14 @@
 
         lax.fori_loop(1, n_sp, step, 0)
 
-    each(
-        lambda d: pl.semaphore_signal(
-            barrier, inc=1, device_id={"sp": lax.rem(sp + d, n_sp)}, device_id_type=MESH
-        )
-    )
-    pl.semaphore_wait(barrier, 2 + n_sp - 1)
+    def tell(sem, d):
+        for to in (lax.rem(sp + d, n_sp), lax.rem(sp + n_sp - d, n_sp)):
+            pl.semaphore_signal(sem, inc=1, device_id={"sp": to}, device_id_type=MESH)
+
+    tell(barrier, 1)
+    pl.semaphore_wait(barrier, 4)
+    rounds = n_sp.bit_length() - 2
+    tell(known.at[0], 1)
 
     def beside(src, dst, ss, rs, to_right):
         return pltpu.make_async_remote_copy(
@@ -112,7 +116,7 @@
         return pl.ds(pl.multiple_of(c * tc + off, 16), size)
 
     def own(c, to_right):
-        rows = rows_of(c, tc)
+        rows = pl.ds(pl.multiple_of(c * tm, 16), tm)
         return beside(
             x.at[rows, :],
             (xl if to_right else xr).at[rows, :],
@@ -122,7 +126,7 @@
         )
 
     def forward(c, to_right):
-        rows = rows_of(c, half, 0 if to_right else half)
+        rows = pl.ds(pl.multiple_of(c * tm + (0 if to_right else half), 16), half)
         return beside(
             (xl if to_right else xr).at[rows, :],
             xo.at[rows, :],
@@ -137,10 +141,12 @@
         own(c, False).wait_recv()
         forward(c, False).start()
 
-    lead = min(2, chunks)
-    for c in range(lead):
+    def send(c):
         own(c, True).start()
         own(c, False).start()
+
+    send(0)
+    send(1)
 
     state[...] = jnp.zeros_like(state)
     run[...] = jnp.zeros_like(run)
@@ -149,25 +155,42 @@
     col = lax.broadcasted_iota(jnp.int32, (BLK, 2 * BLK), 1)
     tri2[...] = jnp.where(row >= lax.rem(col, BLK), 1.0, 0.0).astype(BF16)
 
+    xn[:, 0:width] = (x[...].astype(F32) * gains[:, pl.ds(pl.multiple_of(me * width, width), width)]).astype(BF16)
+    for copy in early:
+        copy.wait()
+
+    def own_wide(k, carry):
+        cs = pl.ds(pl.multiple_of(k * width, width), width)
+        accc[:, cs] = dot(xn[:, 0:width], wv[k + 3, 0:width, :])
+        return carry
+
+    def own_narrow(k, carry):
+        part3[k] = dot(xn[:, 0:width], wv[k, 0:width, :])
+        return carry
+
+    lax.fori_loop(0, 3, own_narrow, 0)
     pass_on(0)
-    if chunks > lead:
-        own(lead, True).start()
-        own(lead, False).start()
+    send(2)
+    lax.fori_loop(0, 4, own_wide, 0)
+    pass_on(1)
+    send(3)
     for copy in first:
         copy.wait()
 
     def chunk(c, carry):
-        @pl.when(c + 1 < chunks)
-        def _():
-            pass_on(c + 1)
-
-        @pl.when(c + 1 + lead < chunks)
-        def _():
-            own(c + 1 + lead, True).start()
-            own(c + 1 + lead, False).start()
-
-        forward(c, True).wait_recv()
-        forward(c, False).wait_recv()
+        def relay(m):
+            @pl.when(m < parts)
+            def _():
+                pass_on(m)
+
+            @pl.when(m + 2 < parts)
+            def _():
+                send(m + 2)
+
+        relay(2 * c + 2)
+        for m in range(2):
+            forward(2 * c + m, True).wait_recv()
+            forward(2 * c + m, False).wait_recv()
 
         rows = rows_of(c, tc)
         total = jnp.zeros((tc, 1), F32)
@@ -175,16 +198,18 @@
             v = piece[rows, :].astype(F32)
             total = total + jnp.sum(v * v, axis=1, keepdims=True)
         scale = lax.rsqrt(total * (1.0 / full) + EPS)
-        for r, piece in enumerate((x, xl, xr, xo)):
+        scales[rows, :] = jnp.broadcast_to(scale, (tc, DK))
+        for r, piece in ((1, xl), (2, xr), (3, xo)):
             g = gains[:, pl.ds(pl.multiple_of(srcs[r] * width, width), width)]
-            v = piece[rows, :].astype(F32) * scale * g
-            xn[rows, r * width : (r + 1) * width] = v.astype(BF16)
+            xn[rows, r * width : (r + 1) * width] = (piece[rows, :].astype(F32) * g).astype(BF16)
 
         def project(k, carry):
-            pr[k] = dot(xn[rows, :], wv[k]).astype(BF16)
+            total = dot(xn[rows, width:], wv[k, width:, :]) + part3[k, rows, :]
+            pr[k] = (total * scales[rows, 0:1]).astype(BF16)
             return carry
 
         lax.fori_loop(0, 3, project, 0)
+        relay(2 * c + 3)
 
         for b in range(tc // BLK):
             lr = slice(b * BLK, (b + 1) * BLK)
@@ -215,6 +240,14 @@
                 part[gr, ln] = dot(sc, v) + dot(qc, sh.astype(BF16), NT)
                 state[h] = jnp.exp(tot) * sh + dot(v, kh, TN)
                 run[:, ln] = runh + tot
+        for k in range(rounds):
+
+            @pl.when(c == k)
+            def _():
+                pl.semaphore_wait(known.at[k], 2)
+                if k + 1 < rounds:
+                    tell(known.at[k + 1], 2 ** (k + 1))
+
         return carry
 
     lax.fori_loop(0, chunks, chunk, 0)
@@ -248,7 +281,9 @@
         copy.wait()
 
     def wide(k, carry):
-        pd[k] = dot(xn[...], wv[k + 3]).astype(BF16)
+        cs = pl.ds(pl.multiple_of(k * width, width), width)
+        total = dot(xn[:, width:], wv[k + 3, width:, :]) + accc[:, cs]
+        pd[k] = (total * scales[:, 0:1]).astype(BF16)
         return carry
 
     lax.fori_loop(0, 2, wide, 0)
@@ -410,7 +445,7 @@
         forward(c, False).wait_send()
         return carry
 
-    lax.fori_loop(0, chunks, finish, 0)
+    lax.fori_loop(0, parts, finish, 0)
 
     def drain(d):
         there(d).wait_send()
@@ -464,6 +499,8 @@
                 v((1, width), F32),
                 v((BLK, 2 * BLK), BF16),
                 v((1, full), F32),
+                v((3, tokens, width), F32),
+                v((tokens, DK), F32),
                 v((tokens, width), F32),
                 v((tokens, width), BF16),
                 v((n_sp, mrows, DK), F32),
@@ -485,10 +522,11 @@
                 v((2, tb, cols), BF16),
                 v((2, tb, cols), BF16),
                 v((2, tb, cols), F32),
+                pltpu.SemaphoreType.REGULAR((4,)),
                 dma((7, 4)),
                 dma((3,)),
             ]
-            + [dma((chunks,))] * 8
+            + [dma((2 * chunks,))] * 8
             + [dma((n_sp,))] * 4
             + [dma] * 6
             + [dma((2,))] * 4,

time: 90.7 us -> 88.8 us (0.979)
  Pallas kernels: 88.4 us -> 86.5 us
    pallas_call x1, Pallas kernels: 88.4 us -> 86.5 us  [body(): pl.pallas_call(lambda *refs: layer(chunks, n_sp, *refs), out_shape=jax.Sh...]
where the time goes in v3:
time: 88.8 us; the launch traced here: 88.6 us
  Pallas kernels  86.5 us (97%)
  local copies, waits for them, and re-layouts  2.09 us (2%)
    pallas_call x1, Pallas kernels, body(): pl.pallas_call(lambda *refs: layer(chunks, n_sp, *refs), out_shape=jax.Sh...  86.5 us
    unnamed x1, local copies, waits for them, and re-layouts  2.09 us

profile of v3, /device:TPU:1, one launch (start us, length us, event | category | flops | bytes accessed | tf_op | source)
XLA Modules:
  0.0 88.6 jit_solution(9917447589637909122)
XLA Ops:
  0.0 86.5 %layer.1 = bf16[192,2048]{1,0:T(8,128)(2,1)} custom-call(bf16[768,512]{1,0:T(8,128)(2,1)} %refs_0_.1, bf16[2048]{0:T(1024)(128)(2,1)} %refs_1_.1, f32[768,512]{1,0:T(8,128)} %refs_2_.1, f32[1,512]{1,0:T(1,128)} %bitcast.2, bf16[3,512]{1,0:T(4,128)(2,1)} %refs_4_.1, bf16[1,128]{1,0:T(2,128)(2,1)} %bitcast.3, f32[4,4,128]{2,1,0:T(4,128)} %refs_6_.1, ...), custom_call_target="tpu_custom_call" | custom-call | tf_op jit(solution)/shard_map/layer/pallas_call | solution.py:481
  86.6 2.1 %copy.19 = bf16[192,2048]{1,0:T(8,128)(2,1)} copy(bf16[192,2048]{1,0:T(8,128)(2,1)} %layer.1) | data formatting | bytes 1572864

commit v4 on v3

--- a/solution.py
+++ b/solution.py
@@ -37,11 +37,11 @@
     ws = refs[8:15]
     wr_in, wc_in, out = refs[15:18]
     (xl, xr, xo, xn, wv, wr, wc, sv, pr, pd, mx, state, run, tri2, gains) = refs[18:33]
-    (part3, scales, part, qs, stf, st, got, dcol, back, sin, rim, rim_in, sb, rec, cvo, accc) = refs[33:49]
-    (po, pp, ra, rb, fl, fr, acc) = refs[49:56]
-    known, wsem, msem, s_or, s_ol, s_fr, s_fl, r_l, r_r, r_oa, r_ob = refs[56:67]
-    s1, r1, s2, r2, rs, rr = refs[67:73]
-    s_a, s_b, r_a, r_b, s_r, s_l, r_fl, r_fr = refs[73:]
+    (kts, runs, snap, part3, scales, part, qs, stf, st, got, dcol, back, sin, rim, rim_in, sb, rec, cvo, accc) = refs[33:52]
+    (po, pp, ra, rb, fl, fr, acc) = refs[52:59]
+    known, wsem, msem, s_or, s_ol, s_fr, s_fl, r_l, r_r, r_oa, r_ob = refs[59:70]
+    s1, r1, s2, r2, rs, rr = refs[70:76]
+    s_a, s_b, r_a, r_b, s_r, s_l, r_fl, r_fr = refs[76:]
     tokens, width = x.shape
     full = 4 * width
     tc = tokens // chunks
@@ -177,6 +177,28 @@
     for copy in first:
         copy.wait()
 
+    def outputs(c, carry):
+        rows = rows_of(c, tc)
+        total = dot(xn[rows, width:], wv[0, width:, :]) + part3[0, rows, :]
+        pr[0, rows, :] = (total * scales[rows, 0:1]).astype(BF16)
+        for b in range(tc // BLK):
+            gr = rows_of(c, BLK, b * BLK)
+            block = c * (tc // BLK) + b
+            for h in range(heads):
+                ln = slice(h * DK, (h + 1) * DK)
+                cum = mx[gr, ln]
+                ref = cum[BLK // 2 - 1 : BLK // 2, :]
+                qraw = pr[0, gr, ln].astype(F32)
+                qt = qraw * sigmoid(qraw) * (DK**-0.5) * jnp.exp(cum - ref)
+                qc = (qt * jnp.exp(ref)).astype(BF16)
+                qs[gr, ln] = (qt * jnp.exp(ref + runs[block, :, ln])).astype(BF16)
+                sc = dot(qt.astype(BF16), kts[gr, ln], NT)
+                ri = lax.broadcasted_iota(jnp.int32, (BLK, BLK), 0)
+                ci = lax.broadcasted_iota(jnp.int32, (BLK, BLK), 1)
+                sc = jnp.where(ri >= ci, sc, 0.0).astype(BF16)
+                part[gr, ln] = dot(sc, pr[2, gr, ln]) + dot(qc, snap[block, h], NT)
+        return carry
+
     def chunk(c, carry):
         def relay(m):
             @pl.when(m < parts)
@@ -205,41 +227,39 @@
 
         def project(k, carry):
             total = dot(xn[rows, width:], wv[k, width:, :]) + part3[k, rows, :]
-            pr[k] = (total * scales[rows, 0:1]).astype(BF16)
+            pr[k, rows, :] = (total * scales[rows, 0:1]).astype(BF16)
             return carry
 
-        lax.fori_loop(0, 3, project, 0)
+        lax.fori_loop(1, 3, project, 0)
         relay(2 * c + 3)
 
         for b in range(tc // BLK):
-            lr = slice(b * BLK, (b + 1) * BLK)
             gr = rows_of(c, BLK, b * BLK)
+            block = c * (tc // BLK) + b
+            runs[block] = run[...]
+            hl = [slice(h * DK, (h + 1) * DK) for h in range(heads)]
+            us = [(1.0 - fmin[:, ln]) * sigmoid(-pr[1, gr, ln].astype(F32)) for ln in hl]
+            lgs = [log_one_minus(u) + sv[gr, ln] for u, ln in zip(us, hl)]
+            his = [lg.astype(BF16) for lg in lgs]
+            los = [(lg - hi.astype(F32)).astype(BF16) for lg, hi in zip(lgs, his)]
+            cums = [dot(tri2[...], jnp.concatenate([a, b], axis=0)) for a, b in zip(his, los)]
             for h in range(heads):
-                ln = slice(h * DK, (h + 1) * DK)
-                u = (1.0 - fmin[:, ln]) * sigmoid(-pr[1, lr, ln].astype(F32))
-                lg = log_one_minus(u) + sv[gr, ln]
-                hi = lg.astype(BF16)
-                lo = (lg - hi.astype(F32)).astype(BF16)
-                cum = dot(tri2[...], jnp.concatenate([hi, lo], axis=0))
+                ln, cum = hl[h], cums[h]
+                mx[gr, ln] = cum
                 ref = cum[BLK // 2 - 1 : BLK // 2, :]
                 tot = cum[BLK - 1 : BLK, :]
-                d = cum - ref
-                qraw = pr[0, lr, ln].astype(F32)
-                qt = qraw * sigmoid(qraw) * (DK**-0.5) * jnp.exp(d)
-                kt = u * jnp.exp(-d)
-                runh = run[:, ln]
-                qc = (qt * jnp.exp(ref)).astype(BF16)
-                qs[gr, ln] = (qt * jnp.exp(ref + runh)).astype(BF16)
+                kt = us[h] * jnp.exp(ref - cum)
+                kts[gr, ln] = kt.astype(BF16)
                 kh = (kt * jnp.exp(tot - ref)).astype(BF16)
-                v = pr[2, lr, ln]
-                sc = dot(qt.astype(BF16), kt.astype(BF16), NT)
-                ri = lax.broadcasted_iota(jnp.int32, (BLK, BLK), 0)
-                ci = lax.broadcasted_iota(jnp.int32, (BLK, BLK), 1)
-                sc = jnp.where(ri >= ci, sc, 0.0).astype(BF16)
                 sh = state[h]
-                part[gr, ln] = dot(sc, v) + dot(qc, sh.astype(BF16), NT)
-                state[h] = jnp.exp(tot) * sh + dot(v, kh, TN)
-                run[:, ln] = runh + tot
+                snap[block, h] = sh.astype(BF16)
+                state[h] = jnp.exp(tot) * sh + dot(pr[2, gr, ln], kh, TN)
+                run[:, ln] = run[:, ln] + tot
+
+        @pl.when(c < chunks - 2)
+        def _():
+            outputs(c, 0)
+
         for k in range(rounds):
 
             @pl.when(c == k)
@@ -286,6 +306,7 @@
         pd[k] = (total * scales[:, 0:1]).astype(BF16)
         return carry
 
+    lax.fori_loop(chunks - 2, chunks, outputs, 0)
     lax.fori_loop(0, 2, wide, 0)
     mx[0:8, :] = jnp.zeros((8, width), F32)
     piece = tokens // 8
@@ -469,7 +490,6 @@
 
     def body(x, ing, wq, wf, wval, wog, wpost, wpre, wcv, fmin, surge, taps, hgain, start, wr, wc, ong):
         tokens, width = x.shape
-        tc = tokens // chunks
         heads = width // DK
         own_rows = DK // n_sp
         rows = heads * own_rows
@@ -492,13 +512,16 @@
                 v((width, full), BF16),
                 v((width, full), BF16),
                 v((tokens, width), F32),
-                v((3, tc, width), BF16),
+                v((3, tokens, width), BF16),
                 v((4, tokens, width), BF16),
                 v((tokens + 8, width), F32),
                 v((heads, DV, DK), F32),
                 v((1, width), F32),
                 v((BLK, 2 * BLK), BF16),
                 v((1, full), F32),
+                v((tokens, width), BF16),
+                v((tokens // BLK, 1, width), F32),
+                v((tokens // BLK, heads, DV, DK), BF16),
                 v((3, tokens, width), F32),
                 v((tokens, DK), F32),
                 v((tokens, width), F32),

time: 88.8 us -> 86.2 us (0.971)
  Pallas kernels: 86.5 us -> 83.3 us
    pallas_call x1, Pallas kernels: 86.5 us -> 83.3 us  [body(): pl.pallas_call(lambda *refs: layer(chunks, n_sp, *refs), out_shape=jax.Sh...]
where the time goes in v4:
time: 86.2 us; the launch traced here: 85.4 us
  Pallas kernels  83.3 us (97%)
  local copies, waits for them, and re-layouts  2.09 us (2%)
    pallas_call x1, Pallas kernels, body(): pl.pallas_call(lambda *refs: layer(chunks, n_sp, *refs), out_shape=jax.Sh...  83.3 us
    unnamed x1, local copies, waits for them, and re-layouts  2.09 us

profile of v4, /device:TPU:1, one launch (start us, length us, event | category | flops | bytes accessed | tf_op | source)
XLA Modules:
  0.0 85.4 jit_solution(10918159957772661995)
XLA Ops:
  0.0 83.3 %layer.1 = bf16[192,2048]{1,0:T(8,128)(2,1)} custom-call(bf16[768,512]{1,0:T(8,128)(2,1)} %refs_0_.1, bf16[2048]{0:T(1024)(128)(2,1)} %refs_1_.1, f32[768,512]{1,0:T(8,128)} %refs_2_.1, f32[1,512]{1,0:T(1,128)} %bitcast.2, bf16[3,512]{1,0:T(4,128)(2,1)} %refs_4_.1, bf16[1,128]{1,0:T(2,128)(2,1)} %bitcast.3, f32[4,4,128]{2,1,0:T(4,128)} %refs_6_.1, ...), custom_call_target="tpu_custom_call" | custom-call | tf_op jit(solution)/shard_map/layer/pallas_call | solution.py:501
  83.3 2.1 %copy.19 = bf16[192,2048]{1,0:T(8,128)(2,1)} copy(bf16[192,2048]{1,0:T(8,128)(2,1)} %layer.1) | data formatting | bytes 1572864

commit v5 on v4

--- a/solution.py
+++ b/solution.py
@@ -38,10 +38,10 @@
     wr_in, wc_in, out = refs[15:18]
     (xl, xr, xo, xn, wv, wr, wc, sv, pr, pd, mx, state, run, tri2, gains) = refs[18:33]
     (kts, runs, snap, part3, scales, part, qs, stf, st, got, dcol, back, sin, rim, rim_in, sb, rec, cvo, accc) = refs[33:52]
-    (po, pp, ra, rb, fl, fr, acc) = refs[52:59]
-    known, wsem, msem, s_or, s_ol, s_fr, s_fl, r_l, r_r, r_oa, r_ob = refs[59:70]
-    s1, r1, s2, r2, rs, rr = refs[70:76]
-    s_a, s_b, r_a, r_b, s_r, s_l, r_fl, r_fr = refs[76:]
+    (po, pp, ra, fl, fr, acc) = refs[52:58]
+    known, wsem, msem, s_or, s_ol, s_fr, s_fl, r_l, r_r, r_oa, r_ob = refs[58:69]
+    s1, r1, s2, r2, rs, rr = refs[69:75]
+    s_a, r_a, s_r, s_l, r_fl, r_fr = refs[75:]
     tokens, width = x.shape
     full = 4 * width
     tc = tokens // chunks
@@ -52,7 +52,6 @@
     own_rows = DK // n_sp
     srows = heads * own_rows
     tb = tokens // 4
-    cols = full // 2
     me = lax.axis_index("tp")
     sp = lax.axis_index("sp")
     right, left, opp = lax.rem(me + 1, 4), lax.rem(me + 3, 4), lax.rem(me + 2, 4)
@@ -174,7 +173,7 @@
     lax.fori_loop(0, 4, own_wide, 0)
     pass_on(1)
     send(3)
-    for copy in first:
+    for copy in first + later:
         copy.wait()
 
     def outputs(c, carry):
@@ -197,6 +196,19 @@
                 ci = lax.broadcasted_iota(jnp.int32, (BLK, BLK), 1)
                 sc = jnp.where(ri >= ci, sc, 0.0).astype(BF16)
                 part[gr, ln] = dot(sc, pr[2, gr, ln]) + dot(qc, snap[block, h], NT)
+        return carry
+
+    def wide(k, rows):
+        cs = pl.ds(pl.multiple_of(k * width, width), width)
+        total = dot(xn[rows, width:], wv[k + 3, width:, :]) + accc[rows, cs]
+        pd[k, rows, :] = (total * scales[rows, 0:1]).astype(BF16)
+
+    def wide_chunk(k, c):
+        wide(k, rows_of(c, tc))
+        return c
+
+    def wide_rest(k, carry):
+        wide(k, pl.ds(2 * tc, tokens - 2 * tc))
         return carry
 
     def chunk(c, carry):
@@ -260,6 +272,10 @@
         def _():
             outputs(c, 0)
 
+        @pl.when((c >= 1) & (c <= 2))
+        def _():
+            lax.fori_loop(0, 4, wide_chunk, c - 1)
+
         for k in range(rounds):
 
             @pl.when(c == k)
@@ -297,17 +313,9 @@
     each(lambda d: there(d).start())
     got[sp] = st[sp]
 
-    for copy in later:
-        copy.wait()
-
-    def wide(k, carry):
-        cs = pl.ds(pl.multiple_of(k * width, width), width)
-        total = dot(xn[:, width:], wv[k + 3, width:, :]) + accc[:, cs]
-        pd[k] = (total * scales[:, 0:1]).astype(BF16)
-        return carry
 
     lax.fori_loop(chunks - 2, chunks, outputs, 0)
-    lax.fori_loop(0, 2, wide, 0)
+    lax.fori_loop(0, 2, wide_rest, 0)
     mx[0:8, :] = jnp.zeros((8, width), F32)
     piece = tokens // 8
 
@@ -343,7 +351,7 @@
     each(lambda d: again(d).start())
     sin[sp] = back[sp]
 
-    lax.fori_loop(2, 4, wide, 0)
+    lax.fori_loop(2, 4, wide_rest, 0)
     rim_copy().wait_recv()
     inside = jnp.where(sp == 0, 0.0, 1.0)
     mx[0:8, :] = rim_in[...] * inside
@@ -358,7 +366,7 @@
 
     lax.fori_loop(0, 8, convolve, 0)
 
-    step = 512 if cols % 512 == 0 else cols
+    step = 512
 
     def conv_part(n, carry):
         cs = pl.ds(pl.multiple_of(n * step, step), step)
@@ -387,77 +395,69 @@
             g = pd[3, rows, ln].astype(F32)
             rec[rows, ln] = (o * (g * sigmoid(g))).astype(BF16)
 
-    def product(owner, side, put):
+    pieces = full // step
+    mid = pieces // 2
+
+    def product(owner, n):
         rows = block_rows(owner)
-
-        def one(n, carry):
-            cs = pl.ds(pl.multiple_of(n * step, step), step)
-            ns = pl.ds(pl.multiple_of(side * cols + n * step, step), step)
-            put(cs, dot(rec[rows, :], wr[:, ns]) + accc[rows, ns])
-            return carry
-
-        lax.fori_loop(0, cols // step, one, 0)
-
-    far_a = beside(po.at[0], ra, s_a, r_a, True)
-    far_b = beside(po.at[1], rb, s_b, r_b, False)
-    near_r = [beside(pp.at[0, s], fl.at[s], s_r.at[s], r_fl.at[s], True) for s in range(2)]
-    near_l = [beside(pp.at[1, s], fr.at[s], s_l.at[s], r_fr.at[s], False) for s in range(2)]
-
-    def store(ref):
-        def put(cs, v):
-            ref[:, cs] = v.astype(BF16)
-
-        return put
-
-    def store_sum(ref, other):
-        def put(cs, v):
-            ref[:, cs] = (v + other[:, cs].astype(F32)).astype(BF16)
-
-        return put
-
-    def keep(side):
-        def put(cs, v):
-            acc[side, :, cs] = v
-
-        return put
-
+        ns = slice(n * step, (n + 1) * step)
+        return dot(rec[rows, :], wr[:, ns]) + accc[rows, ns]
+
+    def far(n):
+        to_right = n < mid
+        return beside(po.at[n], ra.at[n], s_a.at[n], r_a.at[n], to_right)
+
+    def near(n, to_right):
+        k = 0 if to_right else 1
+        return beside(
+            pp.at[k, n],
+            (fl if to_right else fr).at[n],
+            (s_r if to_right else s_l).at[n],
+            (r_fl if to_right else r_fr).at[n],
+            to_right,
+        )
+
+    order = [k // 2 if k % 2 == 0 else mid + k // 2 for k in range(pieces)]
     mix_heads(opp)
-    product(opp, 0, store(po.at[0]))
-    far_a.start()
-    product(opp, 1, store(po.at[1]))
-    far_b.start()
+    for n in order:
+        po[n] = product(opp, n).astype(BF16)
+        far(n).start()
     mix_heads(right)
-    product(right, 1, store(pp.at[0, 1]))
-    near_r[1].start()
+    for n in range(mid, pieces):
+        pp[0, n] = product(right, n).astype(BF16)
+        near(n, True).start()
     mix_heads(left)
-    product(left, 0, store(pp.at[1, 0]))
-    near_l[0].start()
+    for n in range(mid):
+        pp[1, n] = product(left, n).astype(BF16)
+        near(n, False).start()
     mix_heads(me)
-    for side in range(2):
-        product(me, side, keep(side))
-    far_a.wait_recv()
-    product(right, 0, store_sum(pp.at[0, 0], ra))
-    near_r[0].start()
-    far_b.wait_recv()
-    product(left, 1, store_sum(pp.at[1, 1], rb))
-    near_l[1].start()
-
+    for n in range(pieces):
+        acc[n] = product(me, n)
+    for n in order:
+        to_right = n < mid
+        owner, k = (right, 0) if to_right else (left, 1)
+        value = product(owner, n)
+        far(n).wait_recv()
+        pp[k, n] = (value + ra[n].astype(F32)).astype(BF16)
+        near(n, to_right).start()
+
+    def add_in(n, to_right):
+        near(n, to_right).wait_recv()
+        acc[n] = acc[n] + (fl if to_right else fr)[n].astype(F32)
+
+    for k in range(mid):
+        add_in(mid + k, True)
+        add_in(k, False)
     sq = jnp.zeros((tb, 1), F32)
-    for side in (1, 0):
-        near_r[side].wait_recv()
-        near_l[side].wait_recv()
-        for n in range(cols // step):
-            cs = slice(n * step, (n + 1) * step)
-            v = acc[side, :, cs] + fl[side, :, cs].astype(F32) + fr[side, :, cs].astype(F32)
-            acc[side, :, cs] = v
-            sq = sq + jnp.sum(v * v, axis=1, keepdims=True)
+    for n in order:
+        add_in(n, n < mid)
+        v = acc[n]
+        sq = sq + jnp.sum(v * v, axis=1, keepdims=True)
     scale = lax.rsqrt(sq * (1.0 / full) + EPS)
     gains[...] = ogain[...].astype(F32).reshape(1, full)
-    for side in range(2):
-        for n in range(cols // step):
-            cs = slice(n * step, (n + 1) * step)
-            gs = slice(side * cols + n * step, side * cols + (n + 1) * step)
-            out[:, gs] = (acc[side, :, cs] * scale * gains[:, gs]).astype(BF16)
+    for n in range(pieces):
+        ns = slice(n * step, (n + 1) * step)
+        out[:, ns] = (acc[n] * scale * gains[:, ns]).astype(BF16)
 
     def finish(c, carry):
         own(c, True).wait_send()
@@ -474,11 +474,10 @@
 
     each(drain)
     rim_copy().wait_send()
-    far_a.wait_send()
-    far_b.wait_send()
-    for s in range(2):
-        near_r[s].wait_send()
-        near_l[s].wait_send()
+    for n in range(pieces):
+        far(n).wait_send()
+        near(n, True).wait_send()
+        near(n, False).wait_send()
 
 
 def solution(mesh):
@@ -496,7 +495,6 @@
         mrows = rows + 2 * heads
         tb = tokens // 4
         full = 4 * width
-        cols = full // 2
         v = pltpu.VMEM
         return pl.pallas_call(
             lambda *refs: layer(chunks, n_sp, *refs),
@@ -538,21 +536,20 @@
                 v((tokens, width), BF16),
                 v((tokens, width), BF16),
                 v((tokens, full), F32),
-                v((2, tb, cols), BF16),
-                v((2, 2, tb, cols), BF16),
-                v((tb, cols), BF16),
-                v((tb, cols), BF16),
-                v((2, tb, cols), BF16),
-                v((2, tb, cols), BF16),
-                v((2, tb, cols), F32),
+                v((4, tb, full // 4), BF16),
+                v((2, 4, tb, full // 4), BF16),
+                v((4, tb, full // 4), BF16),
+                v((4, tb, full // 4), BF16),
+                v((4, tb, full // 4), BF16),
+                v((4, tb, full // 4), F32),
                 pltpu.SemaphoreType.REGULAR((4,)),
                 dma((7, 4)),
                 dma((3,)),
             ]
             + [dma((2 * chunks,))] * 8
             + [dma((n_sp,))] * 4
-            + [dma] * 6
-            + [dma((2,))] * 4,
+            + [dma] * 2
+            + [dma((4,))] * 6,
             compiler_params=pltpu.CompilerParams(
                 collective_id=0, has_side_effects=True, vmem_limit_bytes=VMEM_LIMIT
             ),

time: 86.2 us -> 85.3 us (0.990)
  no operation moved by 1% of the time
where the time goes in v5:
time: 85.3 us; the launch traced here: 85.1 us
  Pallas kernels  83 us (97%)
  local copies, waits for them, and re-layouts  2.09 us (2%)
    pallas_call x1, Pallas kernels, body(): pl.pallas_call(lambda *refs: layer(chunks, n_sp, *refs), out_shape=jax.Sh...  83 us
    unnamed x1, local copies, waits for them, and re-layouts  2.09 us

profile of v5, /device:TPU:1, one launch (start us, length us, event | category | flops | bytes accessed | tf_op | source)
XLA Modules:
  0.0 85.1 jit_solution(2327336821150493898)
XLA Ops:
  0.0 83.0 %layer.1 = bf16[192,2048]{1,0:T(8,128)(2,1)} custom-call(bf16[768,512]{1,0:T(8,128)(2,1)} %refs_0_.1, bf16[2048]{0:T(1024)(128)(2,1)} %refs_1_.1, f32[768,512]{1,0:T(8,128)} %refs_2_.1, f32[1,512]{1,0:T(1,128)} %bitcast.2, bf16[3,512]{1,0:T(4,128)(2,1)} %refs_4_.1, bf16[1,128]{1,0:T(2,128)(2,1)} %bitcast.3, f32[4,4,128]{2,1,0:T(4,128)} %refs_6_.1, ...), custom_call_target="tpu_custom_call" | custom-call | tf_op jit(solution)/shard_map/layer/pallas_call | solution.py:499
  83.0 2.1 %copy.19 = bf16[192,2048]{1,0:T(8,128)(2,1)} copy(bf16[192,2048]{1,0:T(8,128)(2,1)} %layer.1) | data formatting | bytes 1572864

commit v6 on v5

--- a/solution.py
+++ b/solution.py
@@ -83,12 +83,23 @@
         lax.fori_loop(1, n_sp, step, 0)
 
     def tell(sem, d):
-        for to in (lax.rem(sp + d, n_sp), lax.rem(sp + n_sp - d, n_sp)):
-            pl.semaphore_signal(sem, inc=1, device_id={"sp": to}, device_id_type=MESH)
+        @pl.when(sp + d < n_sp)
+        def _():
+            pl.semaphore_signal(sem, inc=1, device_id={"sp": sp + d}, device_id_type=MESH)
+
+        @pl.when(sp >= d)
+        def _():
+            pl.semaphore_signal(sem, inc=1, device_id={"sp": sp - d}, device_id_type=MESH)
+
+    def beyond(d):
+        return jnp.where(sp + d < n_sp, 1, 0) + jnp.where(sp >= d, 1, 0)
+
+    def hear(sem, d):
+        pl.semaphore_wait(sem, beyond(d))
 
     tell(barrier, 1)
-    pl.semaphore_wait(barrier, 4)
-    rounds = n_sp.bit_length() - 2
+    pl.semaphore_wait(barrier, 2 + beyond(1))
+    rounds = n_sp.bit_length() - 1
     tell(known.at[0], 1)
 
     def beside(src, dst, ss, rs, to_right):
@@ -176,6 +187,9 @@
     for copy in first + later:
         copy.wait()
 
+    hear(known.at[0], 1)
+    tell(known.at[1], 2)
+
     def outputs(c, carry):
         rows = rows_of(c, tc)
         total = dot(xn[rows, width:], wv[0, width:, :]) + part3[0, rows, :]
@@ -183,19 +197,24 @@
         for b in range(tc // BLK):
             gr = rows_of(c, BLK, b * BLK)
             block = c * (tc // BLK) + b
-            for h in range(heads):
-                ln = slice(h * DK, (h + 1) * DK)
-                cum = mx[gr, ln]
-                ref = cum[BLK // 2 - 1 : BLK // 2, :]
-                qraw = pr[0, gr, ln].astype(F32)
-                qt = qraw * sigmoid(qraw) * (DK**-0.5) * jnp.exp(cum - ref)
-                qc = (qt * jnp.exp(ref)).astype(BF16)
-                qs[gr, ln] = (qt * jnp.exp(ref + runs[block, :, ln])).astype(BF16)
-                sc = dot(qt.astype(BF16), kts[gr, ln], NT)
-                ri = lax.broadcasted_iota(jnp.int32, (BLK, BLK), 0)
-                ci = lax.broadcasted_iota(jnp.int32, (BLK, BLK), 1)
-                sc = jnp.where(ri >= ci, sc, 0.0).astype(BF16)
-                part[gr, ln] = dot(sc, pr[2, gr, ln]) + dot(qc, snap[block, h], NT)
+            hl = [slice(h * DK, (h + 1) * DK) for h in range(heads)]
+            cums = [mx[gr, ln] for ln in hl]
+            refs_h = [cum[BLK // 2 - 1 : BLK // 2, :] for cum in cums]
+            raws = [pr[0, gr, ln].astype(F32) for ln in hl]
+            qts = [
+                qraw * sigmoid(qraw) * (DK**-0.5) * jnp.exp(cum - ref)
+                for qraw, cum, ref in zip(raws, cums, refs_h)
+            ]
+            qcs = [(qt * jnp.exp(ref)).astype(BF16) for qt, ref in zip(qts, refs_h)]
+            ri = lax.broadcasted_iota(jnp.int32, (BLK, BLK), 0)
+            ci = lax.broadcasted_iota(jnp.int32, (BLK, BLK), 1)
+            scs = [dot(qt.astype(BF16), kts[gr, ln], NT) for qt, ln in zip(qts, hl)]
+            crs = [dot(qc, snap[block, h], NT) for h, qc in enumerate(qcs)]
+            scs = [jnp.where(ri >= ci, sc, 0.0).astype(BF16) for sc in scs]
+            outs = [dot(sc, pr[2, gr, ln]) + cr for sc, ln, cr in zip(scs, hl, crs)]
+            for h, ln in enumerate(hl):
+                qs[gr, ln] = (qts[h] * jnp.exp(refs_h[h] + runs[block, :, ln])).astype(BF16)
+                part[gr, ln] = outs[h]
         return carry
 
     def wide(k, rows):
@@ -276,11 +295,11 @@
         def _():
             lax.fori_loop(0, 4, wide_chunk, c - 1)
 
-        for k in range(rounds):
-
-            @pl.when(c == k)
+        for k in range(1, rounds):
+
+            @pl.when(c == k - 1)
             def _():
-                pl.semaphore_wait(known.at[k], 2)
+                hear(known.at[k], 2**k)
                 if k + 1 < rounds:
                     tell(known.at[k + 1], 2 ** (k + 1))
 
@@ -542,7 +561,7 @@
                 v((4, tb, full // 4), BF16),
                 v((4, tb, full // 4), BF16),
                 v((4, tb, full // 4), F32),
-                pltpu.SemaphoreType.REGULAR((4,)),
+                pltpu.SemaphoreType.REGULAR((5,)),
                 dma((7, 4)),
                 dma((3,)),
             ]

time: 85.3 us -> 84.9 us (level)
  no operation moved by 1% of the time
where the time goes in v6:
time: 84.9 us; the launch traced here: 84.7 us
  Pallas kernels  82.6 us (97%)
  local copies, waits for them, and re-layouts  2.09 us (2%)
    pallas_call x1, Pallas kernels, body(): pl.pallas_call(lambda *refs: layer(chunks, n_sp, *refs), out_shape=jax.Sh...  82.6 us
    unnamed x1, local copies, waits for them, and re-layouts  2.09 us

profile of v6, /device:TPU:1, one launch (start us, length us, event | category | flops | bytes accessed | tf_op | source)
XLA Modules:
  0.0 84.7 jit_solution(6343681789765945362)
XLA Ops:
  0.0 82.6 %layer.1 = bf16[192,2048]{1,0:T(8,128)(2,1)} custom-call(bf16[768,512]{1,0:T(8,128)(2,1)} %refs_0_.1, bf16[2048]{0:T(1024)(128)(2,1)} %refs_1_.1, f32[768,512]{1,0:T(8,128)} %refs_2_.1, f32[1,512]{1,0:T(1,128)} %bitcast.2, bf16[3,512]{1,0:T(4,128)(2,1)} %refs_4_.1, bf16[1,128]{1,0:T(2,128)(2,1)} %bitcast.3, f32[4,4,128]{2,1,0:T(4,128)} %refs_6_.1, ...), custom_call_target="tpu_custom_call" | custom-call | tf_op jit(solution)/shard_map/layer/pallas_call | solution.py:518
  82.6 2.1 %copy.19 = bf16[192,2048]{1,0:T(8,128)(2,1)} copy(bf16[192,2048]{1,0:T(8,128)(2,1)} %layer.1) | data formatting | bytes 1572864
